TPU v7x, 256 devices: a whole 4x4x8 slice. The times are simulated.
256 devices in a mesh: sp: 64 (over z, y, core), tp: 4 (over x).
Axes of the slice: x: 4, y: 4, z: 8, core: 2. Of those that a mesh axis runs over, the one named last changes fastest.
Arguments:
- query_a: bfloat16 [8192, 1536], P('sp', 'tp'), may hold values from -400 to 400
- query_b: bfloat16 [8192, 2048], P('sp', 'tp'), may hold values from -400 to 400
- latent: bfloat16 [8192, 512], P(('sp', 'tp')), may hold values from -6 to 6
- rope_key: bfloat16 [8192, 64], P(('sp', 'tp')), may hold values from -6 to 6
- latent_gain: float32 [512], replicated, may hold values from 0.1 to 1.9
- key_a_weight: bfloat16 [512, 1024], P(None, 'tp'), may hold values from -0.25 to 0.25
- value_a_weight: bfloat16 [512, 1024], P(None, 'tp'), may hold values from -0.25 to 0.25
- key_b_weight: bfloat16 [512, 1024], P(None, 'tp'), may hold values from -0.25 to 0.25
- value_b_weight: bfloat16 [512, 1024], P(None, 'tp'), may hold values from -0.25 to 0.25
- out_a_weight: bfloat16 [1024, 2048], P('tp'), may hold values from -0.25 to 0.25
- out_b_weight: bfloat16 [1024, 2048], P('tp'), may hold values from -0.25 to 0.25
- residual: bfloat16 [8192, 2048], P(('sp', 'tp')), may hold values from -6 to 6
- ffn_gain: float32 [2048], replicated, may hold values from 0.1 to 1.9
- routes: int32 [8192, 2], P(('sp', 'tp')), may hold values from 0 to 63, all different within a row; in each aligned block of 32 rows (0 to 31, 32 to 63, ...) at most 2 rows name the same one
- route_weight: float32 [8192, 2], P(('sp', 'tp')), may hold values from 0.2 to 1
- expert_gate: bfloat16 [64, 2048, 3072], P('sp', None, 'tp'), may hold values from -0.125 to 0.125
- expert_up: bfloat16 [64, 2048, 3072], P('sp', None, 'tp'), may hold values from -0.125 to 0.125
- expert_down: bfloat16 [64, 3072, 2048], P('sp', 'tp'), may hold values from -0.109375 to 0.109375
Outputs:
- layer_out: bfloat16 [8192, 2048], P(('sp', 'tp'))
Inputs may be any that keep to these rules, and one draw needn't show every extreme that they name: `routes`: the 2 experts of a row differ. Among the 32 rows of one device no expert is named more than 2 times, a bound that some block reaches in some devices' rows.
All inputs are finite; a program needn't handle non-finite values.
Results may differ from a plain program's by a relative error of at most 0.019.
The roundings to bfloat16 on the way count: a program that leaves them out, or rounds other values in their place, can miss the bound.
Values may be sent and summed in bfloat16 or wider, within the bound.
A program may use at most 128 MiB of HBM per device.

v0:
```python
import jax
import jax.numpy as jnp
from jax import lax
from jax.sharding import PartitionSpec as P

from jax.experimental import pallas as pl
from jax.experimental.pallas import tpu as pltpu


NOPE_A = 128
VAL_A = 128
NOPE_B = 64
VAL_B = 64
TOP = 2


epsilon = 1e-06
base_theta = 500000.0
masked_score = -1e30


def rms_scale(values, scales):
    floats = values.astype(jnp.float32)
    scaled = floats * lax.rsqrt(jnp.mean(floats * floats, axis=-1, keepdims=True) + epsilon)
    return (scaled * scales).astype(jnp.bfloat16)


def angle_tables(positions, rotary_width):
    inverse = jnp.power(
        jnp.float32(base_theta), -jnp.arange(0, rotary_width, 2, dtype=jnp.float32) / rotary_width
    )
    angles = positions.astype(jnp.float32)[:, None] * inverse[None, :]
    return (jnp.cos(angles), jnp.sin(angles))


def rotate(values, cosine, sine_table):
    middle = cosine.shape[-1]
    first_half = values[..., :middle].astype(jnp.float32)
    second_half = values[..., middle:].astype(jnp.float32)
    turned = jnp.concatenate(
        [
            first_half * cosine - second_half * sine_table,
            second_half * cosine + first_half * sine_table,
        ],
        axis=-1,
    )
    return turned.astype(jnp.bfloat16)


LOG2E = 1.4426950408889634
MESH_ID = pl.DeviceIdType.MESH
NZ, NY, NX = 8, 4, 4


def place():
    sp = lax.axis_index("sp")
    return sp // 8, (sp // 2) % 4, sp % 2, lax.axis_index("tp")


def send(src, dst, send_sem, recv_sem, z, y, c, x):
    return pltpu.make_async_remote_copy(
        src_ref=src,
        dst_ref=dst,
        send_sem=send_sem,
        recv_sem=recv_sem,
        device_id=(z * 8 + y * 2 + c, x),
        device_id_type=MESH_ID,
    )


def nt_dot(a, b):
    return lax.dot_general(a, b, (((1,), (1,)), ((), ())), preferred_element_type=jnp.float32)


def attention_kernel(
    lat_ref, q_ref, ka_ref, kb_ref, va_ref, vb_ref, oa_ref, ob_ref, res_ref, hid_ref,
    latg, qg, w, wo, k_a, k_b0, k_b1, val, scores, o_out, o_in, st_out, st_in, mg, mg_in, pj, pj_in,
    w_sem, zs, zr, xs, xr, ms, mr, qs, qr, os_, or_, ss, sr, gs, gr, ps, pr,
):
    z, y, c, x = place()
    mate = 1 - c
    low = pl.multiple_of(c * 128, 128)
    high = pl.multiple_of(mate * 128, 128)

    loads = [
        pltpu.make_async_copy(r.at[:, pl.ds(low, 128)], w.at[:, pl.ds(i * 128, 128)], w_sem.at[i])
        for i, r in enumerate((ka_ref, kb_ref, va_ref, vb_ref))
    ]
    for i, at in enumerate((low, high)):
        for j, r in enumerate((oa_ref, ob_ref)):
            loads.append(
                pltpu.make_async_copy(
                    r.at[pl.ds(at, 128), :], wo.at[i, pl.ds(j * 128, 128)], w_sem.at[4 + 2 * i + j]
                )
            )
    for load in loads:
        load.start()

    barrier = pltpu.get_barrier_semaphore()

    def greet(pz, py, pc, px):
        pl.semaphore_signal(
            barrier, inc=1, device_id=(pz * 8 + py * 2 + pc, px), device_id_type=MESH_ID
        )

    for d in range(1, NZ):
        greet((z + d) % NZ, y, c, x)
    for d in range(1, NX):
        greet(z, y, c, (x + d) % NX)
    for dy in range(NY):
        for dc in range(2):
            if dy or dc:
                greet(z, (y + dy) % NY, (c + dc) % 2, x)
    pl.semaphore_wait(barrier, NZ - 1 + NX - 1 + 2 * NY - 1)

    own_rows = pl.ds(pl.multiple_of(c * 128 + x * 32, 32), 32)
    core_rows = pl.ds(low, 128)
    sends = []

    z_sends = [None]
    for d in range(1, NZ):
        z_sends.append(
            send(lat_ref, latg.at[d, own_rows], zs.at[d], zr.at[d], (z + d) % NZ, y, c, x)
        )
    for d in (4, 3, 5, 2, 6, 1, 7):
        z_sends[d].start()
    latg[0, own_rows] = lat_ref[...]

    def x_send(d, dx):
        src = lat_ref if d == 0 else latg.at[d, own_rows]
        return send(src, latg.at[d, own_rows], xs.at[d, dx], xr.at[d, dx], z, y, c, (x + dx) % NX)

    x_sends = [[x_send(d, dx) for dx in range(1, NX)] for d in range(NZ)]
    for dx in range(3):
        x_sends[0][dx].start()

    q_sends = []
    for dy in (2, 1, 3, 0):
        for dc in range(2):
            if dy == 0 and dc == 0:
                continue
            pc = (c + dc) % 2
            q_sends.append(
                send(
                    q_ref.at[pc], qg.at[dy, core_rows], qs.at[dy, dc], qr.at[dy, dc],
                    z, (y + dy) % NY, pc, x,
                )
            )
            q_sends[-1].start()
    qg[0, core_rows] = q_ref[c]

    order = (1, 7, 2, 6, 3, 5, 4)
    for d in order:
        z_sends[d].wait_recv()
        for dx in range(3):
            x_sends[d][dx].start()
    m_sends = [
        send(latg.at[d, core_rows], latg.at[d, core_rows], ms.at[d], mr.at[d], z, y, mate, x)
        for d in range(NZ)
    ]
    for d in (0,) + order:
        for dx in range(3):
            x_sends[d][dx].wait_recv()
        m_sends[d].start()

    for load in loads[:4]:
        load.wait()
    lane = lax.broadcasted_iota(jnp.int32, (256, 128), 1)
    for d in (0,) + order:
        m_sends[d].wait_recv()
        block = latg[d]
        made = jnp.dot(block[:, :512], w[...], preferred_element_type=jnp.float32)
        made = made.astype(jnp.bfloat16)
        turned = block[:, 512:]
        b = made[:, 128:256]
        k_a[d, :, :128] = made[:, :128]
        k_a[d, :, 128:] = turned
        k_b0[d] = jnp.where(lane < 64, b, turned)
        k_b1[d] = jnp.where(lane < 64, turned, b)
        val[d] = made[:, 256:]
    for s in q_sends:
        s.wait_recv()

    factors = (LOG2E * 192**-0.5, LOG2E * 128**-0.5, LOG2E * 128**-0.5)
    row = lax.broadcasted_iota(jnp.int32, (256, 256), 0)
    col = lax.broadcasted_iota(jnp.int32, (256, 256), 1)

    def raw_scores(dy, d):
        q = qg[dy]
        return (
            nt_dot(q[:, :256], k_a[d]),
            nt_dot(q[:, 256:384], k_b0[d]),
            nt_dot(q[:, 384:], k_b1[d]),
        )

    def attend(dy, _):
        chip = (y - dy + NY) % NY
        allowed = row + (chip - y) * 256 >= col
        tops = []
        for h, s in enumerate(raw_scores(dy, 0)):
            s = jnp.where(allowed, s, -1e30)
            scores[h, 0] = s
            tops.append(jnp.maximum(s[:, :128], s[:, 128:]))

        def first(d, tops):
            new = []
            for h, s in enumerate(raw_scores(dy, d)):
                scores[h, d] = s
                new.append(jnp.maximum(tops[h], jnp.maximum(s[:, :128], s[:, 128:])))
            return tuple(new)

        tops = lax.fori_loop(1, z + 1, first, tuple(tops))
        tops = [jnp.max(t, axis=1, keepdims=True) for t in tops]

        def second(d, carried):
            new = []
            v = val[d]
            for h in range(3):
                total, acc = carried[h]
                p = jnp.exp2((scores[h, d] - tops[h]) * factors[h])
                total = total + (p[:, :128] + p[:, 128:])
                vh = v[:, :128] if h == 0 else v[:, 128:]
                acc = acc + jnp.dot(
                    p.astype(jnp.bfloat16), vh, preferred_element_type=jnp.float32
                )
                new.append((total, acc))
            return tuple(new)

        zero = jnp.zeros((256, 128), jnp.float32)
        done = lax.fori_loop(0, z + 1, second, ((zero, zero),) * 3)
        outs, lses = [], []
        for h in range(3):
            total = jnp.sum(done[h][0], axis=1, keepdims=True)
            outs.append(done[h][1] / total)
            lses.append(tops[h] * factors[h] + jnp.log2(total))
        o_out[dy, :, :128] = outs[0].astype(jnp.bfloat16)
        o_out[dy, :, 128:] = jnp.where(lane < 64, outs[1], outs[2]).astype(jnp.bfloat16)
        stats = jnp.where(lane == 0, lses[0], jnp.where(lane == 1, lses[1], lses[2]))
        st_out[dy] = jnp.transpose(stats)[:8]
        return 0

    def o_send(dy):
        return send(
            o_out.at[dy], o_in.at[dy], os_.at[dy], or_.at[dy], z, (y - dy + NY) % NY, c, x
        ), send(st_out.at[dy], st_in.at[dy], ss.at[dy], sr.at[dy], z, (y - dy + NY) % NY, c, x)

    o_sends = []
    for dy in (2, 1, 3, 0):
        attend(dy, 0)
        if dy:
            o_sends.extend(o_send(dy))
            for s in o_sends[-2:]:
                s.start()
    for s in o_sends:
        s.wait_recv()

    lse = [jnp.transpose(st_out[0])] + [jnp.transpose(st_in[dy]) for dy in range(1, NY)]
    top = jnp.maximum(jnp.maximum(lse[0], lse[1]), jnp.maximum(lse[2], lse[3]))
    weights = [jnp.exp2(v - top) for v in lse]
    inv = 1.0 / (weights[0] + weights[1] + weights[2] + weights[3])
    sum_a = jnp.zeros((256, 128), jnp.float32)
    sum_b = jnp.zeros((256, 128), jnp.float32)
    for dy in range(NY):
        part = (o_out[0] if dy == 0 else o_in[dy]).astype(jnp.float32)
        wt = weights[dy] * inv
        sum_a = sum_a + part[:, :128] * wt[:, 0:1]
        sum_b = sum_b + part[:, 128:] * jnp.where(lane < 64, wt[:, 1:2], wt[:, 2:3])
    mg[:, :128] = sum_a.astype(jnp.bfloat16)
    mg[:, 128:] = sum_b.astype(jnp.bfloat16)
    swap = send(mg.at[pl.ds(high, 128)], mg_in, gs, gr, z, y, mate, x)
    swap.start()
    for load in loads[4:]:
        load.wait()
    swap.wait_recv()
    made = jnp.dot(mg[core_rows], wo[0], preferred_element_type=jnp.float32)
    made = made + jnp.dot(mg_in[...], wo[1], preferred_element_type=jnp.float32)
    pj[...] = made.astype(jnp.bfloat16)
    p_sends = []
    for dx in (2, 1, 3):
        to = (x + dx) % NX
        p_sends.append(
            send(
                pj.at[pl.ds(pl.multiple_of(to * 32, 32), 32)], pj_in.at[dx], ps.at[dx], pr.at[dx],
                z, y, c, to,
            )
        )
        p_sends[-1].start()
    total = pj[pl.ds(pl.multiple_of(x * 32, 32), 32)].astype(jnp.float32)
    for s in p_sends:
        s.wait_recv()
    for dx in range(1, NX):
        total = total + pj_in[dx].astype(jnp.float32)
    hid_ref[...] = (res_ref[...].astype(jnp.float32) + total).astype(jnp.bfloat16)

    for s in z_sends[1:] + [s for part in x_sends for s in part] + m_sends + q_sends:
        s.wait_send()
    for s in o_sends + [swap] + p_sends:
        s.wait_send()


def attention(latent_rows, queries, weights, residual):
    vm = pl.BlockSpec(memory_space=pltpu.VMEM)
    hbm = pl.BlockSpec(memory_space=pl.ANY)
    bf, f32 = jnp.bfloat16, jnp.float32
    dma = pltpu.SemaphoreType.DMA
    return pl.pallas_call(
        attention_kernel,
        out_shape=jax.ShapeDtypeStruct(residual.shape, bf),
        in_specs=[vm, vm] + [hbm] * 6 + [vm],
        out_specs=vm,
        scratch_shapes=[
            pltpu.VMEM((8, 256, 640), bf),
            pltpu.VMEM((4, 256, 512), bf),
            pltpu.VMEM((512, 512), bf),
            pltpu.VMEM((2, 256, 2048), bf),
            pltpu.VMEM((8, 256, 256), bf),
            pltpu.VMEM((8, 256, 128), bf),
            pltpu.VMEM((8, 256, 128), bf),
            pltpu.VMEM((8, 256, 256), bf),
            pltpu.VMEM((3, 8, 256, 256), f32),
            pltpu.VMEM((4, 256, 256), bf),
            pltpu.VMEM((4, 256, 256), bf),
            pltpu.VMEM((4, 8, 256), f32),
            pltpu.VMEM((4, 8, 256), f32),
            pltpu.VMEM((256, 256), bf),
            pltpu.VMEM((128, 256), bf),
            pltpu.VMEM((128, 2048), bf),
            pltpu.VMEM((4, 32, 2048), bf),
            dma((8,)),
            dma((8,)), dma((8,)),
            dma((8, 4)), dma((8, 4)),
            dma((8,)), dma((8,)),
            dma((4, 2)), dma((4, 2)),
            dma((4,)), dma((4,)),
            dma((4,)), dma((4,)),
            dma, dma,
            dma((4,)), dma((4,)),
        ],
        compiler_params=pltpu.CompilerParams(
            collective_id=0, has_side_effects=True, vmem_limit_bytes=48 * 1024 * 1024
        ),
        cost_estimate=pl.CostEstimate(flops=8 * 10**9, bytes_accessed=8 * 10**6, transcendentals=0),
    )(latent_rows, queries, *weights, residual)


def core_queries(query_a, query_b, cosine, sine_table):
    rows = query_a.shape[0]
    a = query_a.reshape(rows, 2, 192)
    b = query_b.reshape(rows, 4, 128)
    turned_a = rotate(a[:, :, NOPE_A:], cosine[:, None, :], sine_table[:, None, :])
    turned_b = rotate(b[:, :, NOPE_B:], cosine[:, None, :], sine_table[:, None, :])
    empty = jnp.zeros((rows, 64), jnp.bfloat16)
    halves = []
    for c in range(2):
        halves.append(
            jnp.concatenate(
                [
                    a[:, c, :NOPE_A], turned_a[:, c], empty,
                    b[:, 2 * c, :NOPE_B], turned_b[:, 2 * c],
                    turned_b[:, 2 * c + 1], b[:, 2 * c + 1, :NOPE_B],
                ],
                axis=-1,
            )
        )
    return jnp.stack(halves)


def body(
    query_a,
    query_b,
    latent,
    rope_key,
    latent_gain,
    key_a_weight,
    value_a_weight,
    key_b_weight,
    value_b_weight,
    out_a_weight,
    out_b_weight,
    residual,
    ffn_gain,
    routes,
    route_weight,
    expert_gate,
    expert_up,
    expert_down,
):
    column_count = lax.axis_size("tp")
    row_count = latent.shape[0]
    span_size = query_a.shape[0]
    rotary_width = rope_key.shape[1]
    own_first = (lax.axis_index("sp") * column_count + lax.axis_index("tp")) * row_count
    query_first = lax.axis_index("sp") * span_size
    last_query = query_first + span_size - 1
    own_cosine, own_sine = angle_tables(
        own_first + jnp.arange(row_count, dtype=jnp.int32), rotary_width
    )
    normed_latent = rms_scale(latent, latent_gain)
    turned_key = rotate(rope_key, own_cosine, own_sine)
    query_cosine, query_sine = angle_tables(
        query_first + jnp.arange(span_size, dtype=jnp.int32), rotary_width
    )
    queries = core_queries(query_a, query_b, query_cosine, query_sine)
    latent_rows = jnp.concatenate([normed_latent, turned_key, turned_key], axis=-1)
    hidden_state = attention(
        latent_rows,
        queries,
        (key_a_weight, key_b_weight, value_a_weight, value_b_weight, out_a_weight, out_b_weight),
        residual,
    )
    normed = rms_scale(hidden_state, ffn_gain)
    model_width = normed.shape[1]
    experts = lax.axis_size("sp")
    capacity = max(2, 2 * TOP * row_count // experts)
    chosen = routes.reshape(-1)
    expert_ids = jnp.arange(experts, dtype=jnp.int32)
    matches = (chosen[:, None] == expert_ids[None, :]).astype(jnp.int32)
    order_rank = jnp.sum((jnp.cumsum(matches, axis=0) - 1) * matches, axis=1)
    slot_index = (chosen * capacity + order_rank).reshape(row_count, TOP)
    slot_ids = jnp.arange(experts * capacity, dtype=jnp.int32)
    selection = jnp.sum(
        (slot_ids[:, None, None] == slot_index[None, :, :]).astype(jnp.bfloat16), axis=2
    )
    outgoing = jnp.dot(selection, normed, preferred_element_type=jnp.float32).astype(jnp.bfloat16)
    outgoing = outgoing.reshape(experts, capacity, model_width)
    portion = lax.all_gather(
        lax.all_to_all(outgoing, "sp", split_axis=0, concat_axis=0, tiled=True),
        "tp",
        axis=1,
        tiled=True,
    )
    portion_shape = portion.shape
    flat_rows = portion.reshape(portion_shape[0] * portion_shape[1], portion_shape[2])
    gate_values = jnp.dot(flat_rows, expert_gate[0], preferred_element_type=jnp.float32)
    up_values = jnp.dot(flat_rows, expert_up[0], preferred_element_type=jnp.float32)
    hidden = (jax.nn.silu(gate_values) * up_values).astype(jnp.bfloat16)
    partial_value = jnp.dot(hidden, expert_down[0], preferred_element_type=jnp.float32).astype(
        jnp.bfloat16
    )
    partials = lax.optimization_barrier(partial_value).astype(jnp.float32).reshape(portion_shape)
    summed = lax.psum_scatter(partials.astype(jnp.bfloat16), "tp", scatter_dimension=1, tiled=True)
    returned = lax.all_to_all(summed, "sp", split_axis=0, concat_axis=0, tiled=True)
    flat_returned = returned.reshape(experts * capacity, model_width)
    expert_mix = jnp.zeros((row_count, model_width), jnp.float32)
    for route_index in range(TOP):
        selector = (slot_index[:, route_index][:, None] == slot_ids[None, :]).astype(jnp.bfloat16)
        picked = jnp.dot(selector, flat_returned, preferred_element_type=jnp.float32)
        expert_mix = expert_mix + route_weight[:, route_index][:, None] * picked
    return (hidden_state.astype(jnp.float32) + expert_mix).astype(jnp.bfloat16)


def solution(mesh):
    placed = (
        P("sp", "tp"),
        P("sp", "tp"),
        P(("sp", "tp"), None),
        P(("sp", "tp"), None),
        P(),
        P(None, "tp"),
        P(None, "tp"),
        P(None, "tp"),
        P(None, "tp"),
        P("tp", None),
        P("tp", None),
        P(("sp", "tp"), None),
        P(),
        P(("sp", "tp"), None),
        P(("sp", "tp"), None),
        P("sp", None, "tp"),
        P("sp", None, "tp"),
        P("sp", "tp", None),
    )
    return jax.shard_map(
        body, mesh=mesh, in_specs=placed, out_specs=P(("sp", "tp"), None), check_vma=False
    )
```

profile of v0, /device:TPU:1, one launch (start us, length us, event | category | flops | bytes accessed | tf_op | source)
XLA Modules:
  0.0 262.7 jit_solution(11549620615049355715)
XLA Ops:
  6.5 0.6 multiply_power_fusion
  7.1 1.3 copy.117
  8.4 0.6 fusion.66
  9.0 1.0 copy.112
  10.1 0.6 slice_convert_fusion.1
  10.7 0.6 fusion.67
  11.3 0.5 add_convert_fusion
  11.8 0.1 copy.119
  11.9 0.8 copy.135
  12.7 0.9 copy.114
  13.6 0.7 copy.133
  14.3 1.5 copy.134
  15.8 1.4 copy.136
  17.2 1.5 copy.132
  18.7 1.4 copy.138
  20.1 1.4 copy.139
  21.5 1.5 copy.137
  23.0 0.6 add_convert_fusion.1
  23.6 0.9 fusion.39
  24.4 0.6 add_rsqrt_fusion.1
  25.0 0.9 multiply_cosine_fusion
  25.9 1.0 fusion.28
  26.9 0.9 fusion.33
  27.8 0.1 fusion.43
  28.0 0.9 concatenate.23
  28.9 1.6 concatenate.24
  30.5 0.9 pad_maximum_fusion.q_ref
  31.4 0.8 fusion.61
  32.2 0.8 fusion.41
  33.1 0.7 concatenate.20.lat_ref
  33.8 0.8 copy-done.1
  34.6 1.2 copy-done.2
  35.8 1.2 copy-done.3
  37.0 0.9 copy-done.4
  38.0 0.9 copy-done.5
  38.9 0.9 copy-done.6
  39.9 0.9 copy-done.7
  40.8 0.9 copy-done.8
  41.7 56.1 %shard_map.172 = bf16[32,2048]{1,0:T(8,128)(2,1)S(1)} custom-call(bf16[32,640]{1,0:T(8,128)(2,1)S(1)} %copy-done.1, bf16[2,128,512]{2,1,0:T(8,128)(2,1)S(1)} %pad_maximum_fusion.q_ref, bf16[512,256]{1,0:T(8,128)(2,1)S(1)} %copy-done.4, bf16[512,256]{1,0:T(8,128)(2,1)S(1)} %copy-done.5, bf16[512,256]{1,0:T(8,128)(2,1)S(1)} %copy-done.6, ...), custom_call_target="tpu_custom_call" | custom-call | flops 8000000000 | bytes 8000000 | tf_op jit(solution)/shard_map/pallas_call | solution.py:306
  97.8 0.1 fusion.29
  98.0 0.1 copy.126
  98.1 0.1 eq.58
  98.2 0.1 fusion.52
  98.3 0.1 reduce_window_sum.11
  98.4 0.2 select_reduce_fusion
  98.5 0.1 reduce_sum.43
  98.7 0.1 copy.127
  98.7 0.1 fusion.62
  98.8 1.1 convolution_convert_fusion
  100.0 2.2 reshape.111
  102.2 35.7 %all_to_all.10 = bf16[64,2,2048]{2,1,0:T(2,128)(2,1)S(1)} all-to-all(bf16[64,2,2048]{2,1,0:T(2,128)(2,1)} %reshape.111), channel_id=1, replica_groups=mesh['sp'=64,'tp'=4] {'sp'}, dimensions={0} | all-to-all | bytes 1048576 | tf_op jit(solution)/shard_map/all_to_all | solution.py:427
  137.9 1.0 copy.128
  138.9 0.0 reduce-scatter.2.cloned.1.call-start
  139.0 29.1 %all-gather.2.cloned.1.call-done = bf16[64,8,2048]{2,0,1:T(8,128)(2,1)} async-done(((bf16[64,2,2048]{2,0,1:T(8,128)(2,1)}), bf16[64,8,2048]{2,0,1:T(8,128)(2,1)}) %all-gather.2.cloned.1.call-update) | async-done | bytes 2097168 | tf_op jit(solution)/shard_map/all_gather | solution.py:426
  168.1 6.2 %fusion.4 = f32[512,768]{1,0:T(8,128)} fusion(bf16[1,2048,768]{2,1,0:T(8,128)(2,1)} %param.33, bf16[64,8,2048]{2,0,1:T(8,128)(2,1)} %all-gather.2.cloned.1.call-done), kind=kOutput, calls=%fused_computation.4 | convolution fusion | flops 1610612736 | bytes 6815744 | tf_op jit(solution)/shard_map/dot_general | solution.py:434
  174.2 8.7 %fusion.6 = bf16[512,2048]{1,0:T(8,128)(2,1)} fusion(bf16[1,768,2048]{2,1,0:T(8,128)(2,1)S(1)} %copy-done, f32[512,768]{1,0:T(8,128)} %fusion.4, bf16[1,2048,768]{2,1,0:T(8,128)(2,1)} %param.34, bf16[64,8,2048]{2,0,1:T(8,128)(2,1)} %all-gather.2.cloned.1.call-done), kind=kOutput, calls=%fused_computation.6 | convolution fusion | flops 3224633344 | bytes 12058624 | tf_op jit(solution)/shard_map/dot_general | solution.py:437
  183.0 4.1 %copy.130 = bf16[64,8,2048]{2,0,1:T(8,128)(2,1)} copy(bf16[64,8,2048]{2,1,0:T(8,128)(2,1)} %bitcast.58) | data formatting | bytes 4194304 | tf_op jit(solution)/shard_map/convert_element_type | solution.py:441
  187.1 32.6 %reduce-scatter.2.cloned.1.call-done = bf16[64,2,2048]{2,0,1:T(8,128)(2,1)} async-done(((bf16[64,8,2048]{2,0,1:T(8,128)(2,1)}), bf16[64,2,2048]{2,0,1:T(8,128)(2,1)}) %reduce-scatter.2.cloned.1.call-update) | async-done | bytes 524304 | tf_op jit(solution)/shard_map/reduce_scatter | solution.py:441
  219.6 2.4 copy.131
  222.0 10.9 %all-to-all-start.1 = ((bf16[64,2,2048]{2,1,0:T(2,128)(2,1)}), bf16[64,2,2048]{2,1,0:T(2,128)(2,1)}, u32[]{:S(2)}, u32[]{:S(2)}) async-start(bf16[64,2,2048]{2,1,0:T(2,128)(2,1)} %copy.131), calls=%async_computation.2 | async-start | bytes 1048576 | tf_op jit(solution)/shard_map/all_to_all | solution.py:442
  233.0 17.6 %all-to-all-done.1 = bf16[64,2,2048]{2,1,0:T(2,128)(2,1)} async-done(((bf16[64,2,2048]{2,1,0:T(2,128)(2,1)}), bf16[64,2,2048]{2,1,0:T(2,128)(2,1)}, u32[]{:S(2)}, u32[]{:S(2)}) %all-to-all-start.1) | async-done | bytes 524320 | tf_op jit(solution)/shard_map/all_to_all | solution.py:442
  250.5 2.0 reshape.113
  252.6 1.3 convolution_multiply_fusion.1
  253.9 2.0 fusion.11
  (31 shorter events, 0.1 us)
Async XLA Ops:
  6.5 167.7 %copy-start = (bf16[1,768,2048]{2,1,0:T(8,128)(2,1)S(1)}, bf16[1,768,2048]{2,1,0:T(8,128)(2,1)}, u32[]{:S(2)}) copy-start(bf16[1,768,2048]{2,1,0:T(8,128)(2,1)} %param.35) | copy-start | bytes 9437188
  6.5 161.5 %all-gather.2.cloned.1.call-start = ((), (), s32[]{:S(2)}) async-start(), calls=%async_computation.3 | async-start | bytes 2621440 | tf_op jit(solution)/shard_map/all_gather | solution.py:426
  14.3 17.1 %copy-start.9 = (bf16[32,64]{1,0:T(8,128)(2,1)S(1)}, bf16[32,64]{1,0:T(8,128)(2,1)}, u32[]{:S(2)}) copy-start(bf16[32,64]{1,0:T(8,128)(2,1)} %param.21) | copy-start | bytes 12292
  14.3 17.1 %copy-start.12 = (f32[32]{0:T(128)S(1)}, f32[32]{0:T(128)}, u32[]{:S(2)}) copy-start(f32[32]{0:T(128)} %multiply_power_fusion) | copy-start | bytes 388
  14.3 17.9 %copy-start.13 = (f32[512]{0:T(512)S(1)}, f32[512]{0:T(512)}, u32[]{:S(2)}) copy-start(f32[512]{0:T(512)} %param.22) | copy-start | bytes 6148
  33.8 0.8 copy-start.1
  34.6 1.2 copy-start.2
  35.8 1.2 copy-start.3
  37.0 0.9 copy-start.4
  38.0 0.9 copy-start.5
  38.9 0.9 copy-start.6
  39.9 0.9 copy-start.7
  40.8 0.9 copy-start.8
  41.7 56.3 %copy-start.11 = (s32[32,2]{0,1:T(2,128)S(1)}, s32[32,2]{0,1:T(2,128)}, u32[]{:S(2)}) copy-start(s32[32,2]{0,1:T(2,128)} %param.31) | copy-start | bytes 772
  41.7 57.1 %copy-start.10 = (f32[2048]{0:T(1024)S(1)}, f32[2048]{0:T(1024)}, u32[]{:S(2)}) copy-start(f32[2048]{0:T(1024)} %param.30) | copy-start | bytes 24580
  138.9 80.7 %reduce-scatter.2.cloned.1.call-start = ((), (), s32[]{:S(2)}) async-start(), calls=%async_computation.4 | async-start | bytes 2621440 | tf_op jit(solution)/shard_map/reduce_scatter | solution.py:441
  187.0 45.9 %copy-start.14 = (f32[32,2]{0,1:T(2,128)S(1)}, f32[32,2]{0,1:T(2,128)}, u32[]{:S(2)}) copy-start(f32[32,2]{0,1:T(2,128)} %param.32) | copy-start | bytes 772
  222.0 28.5 %all-to-all-start.1 = ((bf16[64,2,2048]{2,1,0:T(2,128)(2,1)}), bf16[64,2,2048]{2,1,0:T(2,128)(2,1)}, u32[]{:S(2)}, u32[]{:S(2)}) async-start(bf16[64,2,2048]{2,1,0:T(2,128)(2,1)} %copy.131), calls=%async_computation.2 | async-start | bytes 1048576 | tf_op jit(solution)/shard_map/all_to_all | solution.py:442
Sparse Core Ops, SparseCore 0:
  139.0 28.9 all-gather.1
  187.2 32.3 reduce-scatter.1
where the time goes:
time: 264 us; the launch traced here: 263 us
  waiting for transfers between devices  79.2 us (30%)
  Pallas kernels  56.1 us (21%)
  local copies, waits for them, and re-layouts  37.9 us (14%)
  blocking collectives  35.7 us (14%)
  matrix products  19.3 us (7%)
  between operations  13.6 us (5%)
  starting transfers between devices  11 us (4%)
  other arithmetic  9.81 us (4%)
    pallas_call x1, Pallas kernels, attention(): pl.pallas_call(attention_kernel, out_shape=jax.ShapeDtypeStruct(residual....  56.1 us
    all_to_all x1, blocking collectives, body(): lax.all_to_all(outgoing, 'sp', split_axis=0, concat_axis=0, tiled=True)  35.7 us
    reduce_scatter x1, waiting for transfers between devices, body(): lax.psum_scatter(partials.astype(jnp.bfloat16), 'tp', scatter_dimension=1...  32.6 us
    all_gather x1, waiting for transfers between devices, body(): lax.all_gather(lax.all_to_all(outgoing, 'sp', split_axis=0, concat_axis=0...  29.1 us
    unnamed x41, local copies, waits for them, and re-layouts  20.5 us
    all_to_all x1, waiting for transfers between devices, body(): lax.all_to_all(summed, 'sp', split_axis=0, concat_axis=0, tiled=True)  17.6 us
    all_to_all x1, starting transfers between devices, body(): lax.all_to_all(summed, 'sp', split_axis=0, concat_axis=0, tiled=True)  10.9 us
    dot_general x1, matrix products, body(): jnp.dot(hidden, expert_down[0], preferred_element_type=jnp.float32)  8.71 us
  transfers between devices with their start and end apart: 3, of which 3 were waited for; matrix products, arithmetic and copies ran while one was open for 0% of the time, Pallas kernels for 0%

commit v1 on v0

v1 whole, which is shorter than its diff:
```python
import jax
import jax.numpy as jnp
import numpy as np
from jax import lax
from jax.experimental import pallas as pl
from jax.experimental.pallas import tpu as pltpu
from jax.sharding import PartitionSpec as P

NZ, NY, NX = 8, 4, 4
TOKENS_PER_SP = 128
ROWS = 32
CHUNKS = 4
WIDE = 512
LOG2E = 1.4426950408889634
EPSILON = 1e-06
BASE_THETA = 500000.0
MASKED = -1e30
MESH_ID = pl.DeviceIdType.MESH
BF, F32 = jnp.bfloat16, jnp.float32


def angle_tables():
    inverse = BASE_THETA ** (-np.arange(0, 64, 2, dtype=np.float64) / 64)
    lanes = np.tile(inverse, 4)[None, :]

    def table(positions):
        angles = positions[:, None] * lanes
        return np.concatenate([np.cos(angles), np.sin(angles)], axis=1).astype(np.float32)

    return table(np.arange(64) * 128.0), table(np.arange(128) * 1.0)


def send(src, dst, send_sem, recv_sem, z, y, c, x):
    return pltpu.make_async_remote_copy(
        src_ref=src,
        dst_ref=dst,
        send_sem=send_sem,
        recv_sem=recv_sem,
        device_id=(z * 8 + y * 2 + c, x),
        device_id_type=MESH_ID,
    )


def dot(a, b):
    return jnp.dot(a, b, preferred_element_type=F32)


def nt_dot(a, b):
    return lax.dot_general(a, b, (((1,), (1,)), ((), ())), preferred_element_type=F32)


def iota(shape, dim):
    return lax.broadcasted_iota(jnp.int32, shape, dim)


def layer_kernel(
    qa_ref, qb_ref, lat_ref, rope_ref, gain_ref, ka_ref, va_ref, kb_ref, vb_ref, oa_ref, ob_ref,
    res_ref, fg_ref, rt_ref, wt_ref, eg_ref, eu_ref, ed_ref, ta_ref, tb_ref,
    out_ref,
    qa, qb, lat, rope, gain, res, fg, rt, wt, ta, tb,
    lat_own, q_own, latg, qg, w, wo, k_a, k_b0, k_b1, val, scores, o_out, o_in, st_out, st_in,
    mg, mg_in, pj, pj_half, pj_in,
    wg, wu, wd, disp, z_in, y_out, x_in, acc_g, acc_u, act, p_out, p_half, p_in, r_sum, ry_in,
    rz_out, rz_in,
    in_sem, w_sem, zs, zr, xs, xr, ms, mr, qs, qr, os_, or_, ss, sr, gs, gr, ps, pr,
    dzs, dzr, dys, dyr, dxs, dxr, rxs, rxr, rys, ryr, rzs, rzr,
):
    sp = lax.axis_index("sp")
    x = lax.axis_index("tp")
    z, y, c = sp // 8, (sp // 2) % 4, sp % 2
    mate = 1 - c
    low = pl.multiple_of(c * 128, 128)
    high = pl.multiple_of(mate * 128, 128)
    up = (x + 1) % NX
    down = (x + NX - 1) % NX

    def zp(d):
        return (z + d + NZ) % NZ

    def yp(d):
        return (y + d + NY) % NY

    def xp(d):
        return (x + d + NX) % NX

    small = [
        pltpu.make_async_copy(src, dst, in_sem.at[i])
        for i, (src, dst) in enumerate(
            (
                (lat_ref, lat), (rope_ref, rope), (gain_ref, gain), (ta_ref, ta), (tb_ref, tb),
                (qa_ref, qa), (qb_ref, qb), (res_ref, res), (fg_ref, fg), (rt_ref, rt), (wt_ref, wt),
            )
        )
    ]
    for load in small:
        load.start()
    loads = [
        pltpu.make_async_copy(r.at[:, pl.ds(low, 128)], w.at[:, pl.ds(i * 128, 128)], w_sem.at[i])
        for i, r in enumerate((ka_ref, kb_ref, va_ref, vb_ref))
    ]
    for i, at in enumerate((low, high)):
        for j, r in enumerate((oa_ref, ob_ref)):
            loads.append(
                pltpu.make_async_copy(
                    r.at[pl.ds(at, 128), :], wo.at[i, pl.ds(j * 128, 128)], w_sem.at[4 + 2 * i + j]
                )
            )
    for i, (src, dst) in enumerate(((eg_ref, wg), (eu_ref, wu), (ed_ref, wd))):
        loads.append(pltpu.make_async_copy(src.at[0], dst, w_sem.at[8 + i]))
    for load in loads:
        load.start()

    barrier = pltpu.get_barrier_semaphore()

    def greet(pz, py, pc, px):
        pl.semaphore_signal(
            barrier, inc=1, device_id=(pz * 8 + py * 2 + pc, px), device_id_type=MESH_ID
        )

    for d in range(1, NZ):
        greet(zp(d), y, c, x)
    for d in range(1, NX):
        greet(z, y, c, xp(d))
    for dy in range(NY):
        for dc in range(2):
            if dy or dc:
                greet(z, yp(dy), (c + dc) % 2, x)

    for load in small[:5]:
        load.wait()
    v = lat[...].astype(F32)
    v = v * lax.rsqrt(jnp.mean(v * v, axis=1, keepdims=True) + EPSILON)
    lat_own[:, :512] = (v * gain[...]).astype(BF)
    base = jnp.sum(jnp.where(iota((64, 256), 0) == sp, ta[...], 0.0), axis=0, keepdims=True)
    cos_a, sin_a = base[:, :128], base[:, 128:]

    def turning(cos_b, sin_b):
        lane = iota(cos_b.shape, 1)
        sine = sin_a * cos_b + cos_a * sin_b
        return cos_a * cos_b - sin_a * sin_b, jnp.where(lane % 64 < 32, -sine, sine)

    def rotated(tile, cosine, sine):
        lane = iota(tile.shape, 1)
        other = jnp.where(
            lane % 64 < 32, pltpu.roll(tile, 96, axis=1), pltpu.roll(tile, 32, axis=1)
        )
        return tile * cosine + other * sine

    own_32 = pl.ds(pl.multiple_of(x * ROWS, ROWS), ROWS)
    cosine, sine = turning(tb[own_32, :128], tb[own_32, 128:])
    twice = (iota((64, 128), 1) % 64 == iota((64, 128), 0)).astype(BF)
    lat_own[:, 512:] = rotated(dot(rope[...], twice), cosine, sine).astype(BF)

    pl.semaphore_wait(barrier, NZ - 1 + NX - 1 + 2 * NY - 1)

    def rows_of(px, at, count):
        return pl.ds(pl.multiple_of(c * 128 + px * ROWS + at, 16), count)

    core_rows = pl.ds(low, 128)
    all_sends = []

    z_sends = [None] + [
        send(lat_own, latg.at[d, rows_of(x, 0, 32)], zs.at[d], zr.at[d], zp(d), y, c, x)
        for d in range(1, NZ)
    ]
    all_sends += z_sends[1:]

    def ring(d):
        own = lat_own if d == 0 else latg.at[d, rows_of(x, 0, 32)]
        to = latg.at[d, rows_of(x, 0, 32)]
        one = latg.at[d, rows_of(down, 0, 16)]
        two = latg.at[d, rows_of(up, 16, 16)]
        return (
            send(own, to, xs.at[d, 0], xr.at[d, 0], z, y, c, up),
            send(own, to, xs.at[d, 1], xr.at[d, 1], z, y, c, down),
            send(one, one, xs.at[d, 2], xr.at[d, 2], z, y, c, up),
            send(two, two, xs.at[d, 3], xr.at[d, 3], z, y, c, down),
        )

    x_sends = [ring(d) for d in range(NZ)]
    for d in range(NZ):
        all_sends += x_sends[d]
    x_sends[0][0].start()
    x_sends[0][1].start()
    for d in (1, 7, 2, 6, 3, 5, 4):
        z_sends[d].start()
    latg[0, rows_of(x, 0, 32)] = lat_own[...]

    small[5].wait()
    small[6].wait()
    cosine, sine = turning(tb[:, :128], tb[:, 128:])
    lane = iota((128, 128), 1)
    t1 = qa[:, 128:256]
    t2 = qa[:, 256:384]
    r1 = rotated(t1.astype(F32), cosine, sine)
    r2 = rotated(t2.astype(F32), cosine, sine)
    mixed = jnp.where(lane < 64, t2.astype(F32), t1.astype(F32))
    q_own[0, :, :128] = qa[:, :128]
    q_own[0, :, 128:256] = jnp.where(lane < 64, r1, 0.0).astype(BF)
    q_own[1, :, :128] = pltpu.roll(mixed, 64, axis=1).astype(BF)
    q_own[1, :, 128:256] = jnp.where(lane < 64, 0.0, r2).astype(BF)
    for h in range(4):
        t = qb[:, h * 128 : h * 128 + 128].astype(F32)
        t = jnp.where(lane < 64, t, rotated(t, cosine, sine))
        if h % 2:
            t = pltpu.roll(t, 64, axis=1)
        q_own[h // 2, :, 256 + (h % 2) * 128 : 384 + (h % 2) * 128] = t.astype(BF)

    q_sends = []
    for dc in range(2):
        pc = (c + dc) % 2
        there = pl.ds(pl.multiple_of(pc * 128, 128), 128)
        one = qg.at[1, pl.ds(pl.multiple_of(pc * 128, 64), 64)]
        one_to = qg.at[2, pl.ds(pl.multiple_of(pc * 128, 64), 64)]
        two = qg.at[3, pl.ds(pl.multiple_of(pc * 128 + 64, 64), 64)]
        two_to = qg.at[2, pl.ds(pl.multiple_of(pc * 128 + 64, 64), 64)]
        q_sends.append(
            (
                send(q_own.at[pc], qg.at[1, core_rows], qs.at[dc, 0], qr.at[dc, 0], z, yp(1), pc, x),
                send(q_own.at[pc], qg.at[3, core_rows], qs.at[dc, 1], qr.at[dc, 1], z, yp(-1), pc, x),
                send(one, one_to, qs.at[dc, 2], qr.at[dc, 2], z, yp(1), c, x),
                send(two, two_to, qs.at[dc, 3], qr.at[dc, 3], z, yp(-1), c, x),
            )
        )
    q_mate = send(q_own.at[mate], qg.at[0, core_rows], qs.at[0, 4], qr.at[0, 4], z, y, mate, x)
    all_sends += q_sends[0] + q_sends[1] + (q_mate,)
    for dc in range(2):
        q_sends[dc][0].start()
        q_sends[dc][1].start()
    q_mate.start()
    qg[0, core_rows] = q_own[c]

    m_sends = [
        send(latg.at[d, core_rows], latg.at[d, core_rows], ms.at[d], mr.at[d], z, y, mate, x)
        for d in range(NZ)
    ]
    all_sends += m_sends

    def forward(d):
        x_sends[d][0].wait_recv()
        x_sends[d][2].start()
        x_sends[d][1].wait_recv()
        x_sends[d][3].start()

    def to_mate(d):
        x_sends[d][2].wait_recv()
        x_sends[d][3].wait_recv()
        m_sends[d].start()

    order = (1, 7, 2, 6, 3, 5, 4)
    steps = (0,) + order
    for i in range(len(steps) + 2):
        if i + 1 < len(steps):
            d = steps[i + 1]
            z_sends[d].wait_recv()
            x_sends[d][0].start()
            x_sends[d][1].start()
        if i < len(steps):
            forward(steps[i])
        if 1 <= i <= len(steps):
            to_mate(steps[i - 1])
        if i in (1, 2):
            dc = i - 1
            q_sends[dc][0].wait_recv()
            q_sends[dc][2].start()
            q_sends[dc][1].wait_recv()
            q_sends[dc][3].start()

    for load in loads[:4]:
        load.wait()
    lane = iota((256, 128), 1)
    for d in steps:
        m_sends[d].wait_recv()
        block = latg[d]
        made = dot(block[:, :512], w[...]).astype(BF)
        turned = block[:, 512:]
        b = made[:, 128:256]
        k_a[d, :, :128] = made[:, :128]
        k_a[d, :, 128:] = turned
        k_b0[d] = jnp.where(lane < 64, b, turned)
        k_b1[d] = jnp.where(lane < 64, turned, b)
        val[d] = made[:, 256:]
    q_mate.wait_recv()
    for dc in range(2):
        q_sends[dc][2].wait_recv()
        q_sends[dc][3].wait_recv()

    factors = (LOG2E * 192**-0.5, LOG2E * 128**-0.5, LOG2E * 128**-0.5)
    row = iota((256, 256), 0)
    col = iota((256, 256), 1)

    def raw_scores(dy, d):
        q = qg[dy]
        return (
            nt_dot(q[:, :256], k_a[d]),
            nt_dot(q[:, 256:384], k_b0[d]),
            nt_dot(q[:, 384:], k_b1[d]),
        )

    def attend(dy):
        allowed = row + (yp(-dy) - y) * 256 >= col
        tops = []
        for h, s in enumerate(raw_scores(dy, 0)):
            s = jnp.where(allowed, s, MASKED)
            scores[h, 0] = s
            tops.append(jnp.maximum(s[:, :128], s[:, 128:]))

        def first(d, tops):
            new = []
            for h, s in enumerate(raw_scores(dy, d)):
                scores[h, d] = s
                new.append(jnp.maximum(tops[h], jnp.maximum(s[:, :128], s[:, 128:])))
            return tuple(new)

        tops = lax.fori_loop(1, z + 1, first, tuple(tops))
        tops = [jnp.max(t, axis=1, keepdims=True) for t in tops]

        def second(d, carried):
            new = []
            values = val[d]
            for h in range(3):
                total, acc = carried[h]
                p = jnp.exp2((scores[h, d] - tops[h]) * factors[h])
                total = total + (p[:, :128] + p[:, 128:])
                acc = acc + dot(p.astype(BF), values[:, :128] if h == 0 else values[:, 128:])
                new.append((total, acc))
            return tuple(new)

        zero = jnp.zeros((256, 128), F32)
        done = lax.fori_loop(0, z + 1, second, ((zero, zero),) * 3)
        outs, lses = [], []
        for h in range(3):
            total = jnp.sum(done[h][0], axis=1, keepdims=True)
            outs.append(done[h][1] / total)
            lses.append(tops[h] * factors[h] + jnp.log2(total))
        o_out[dy, :, :128] = outs[0].astype(BF)
        o_out[dy, :, 128:] = jnp.where(lane < 64, outs[1], outs[2]).astype(BF)
        stats = jnp.where(lane == 0, lses[0], jnp.where(lane == 1, lses[1], lses[2]))
        st_out[dy] = jnp.transpose(stats)[:8]

    o_sends = []
    for dy in (2, 1, 3, 0):
        attend(dy)
        if dy:
            o_sends += [
                send(o_out.at[dy], o_in.at[dy], os_.at[dy], or_.at[dy], z, yp(-dy), c, x),
                send(st_out.at[dy], st_in.at[dy], ss.at[dy], sr.at[dy], z, yp(-dy), c, x),
            ]
            o_sends[-2].start()
            o_sends[-1].start()
    all_sends += o_sends

    for load in small[7:]:
        load.wait()
    eye = iota((32, 32), 0) == iota((32, 32), 1)
    before = iota((32, 32), 1) < iota((32, 32), 0)
    after = iota((32, 32), 0) < iota((32, 32), 1)
    chosen = rt[...]
    row_e = [chosen[k : k + 1].astype(F32) for k in range(2)]
    col_e = [jnp.sum(jnp.where(eye, e, 0.0), axis=1, keepdims=True) for e in row_e]
    share = wt[...]
    col_w = [
        jnp.sum(jnp.where(eye, share[k : k + 1], 0.0), axis=1, keepdims=True) for k in range(2)
    ]

    def slot(e, rank):
        e = e.astype(jnp.int32)
        dz = (e // 8 - z + NZ) % NZ
        dy = ((e // 2) % 4 - y + NY) % NY
        dc = (e % 2 - c + 2) % 2
        return dz * 16 + dy * 4 + dc * 2 + rank.astype(jnp.int32)

    row_slot, col_slot = [], []
    for k in range(2):
        rank_row = jnp.zeros((1, 32), F32)
        rank_col = jnp.zeros((32, 1), F32)
        for o in range(2):
            same = (col_e[o] == row_e[k]) & after
            rank_row = rank_row + jnp.sum(jnp.where(same, 1.0, 0.0), axis=0, keepdims=True)
            same = (row_e[o] == col_e[k]) & before
            rank_col = rank_col + jnp.sum(jnp.where(same, 1.0, 0.0), axis=1, keepdims=True)
        row_slot.append(slot(row_e[k], rank_row))
        col_slot.append(slot(col_e[k], rank_col))
    s_row = iota((128, 32), 0)
    chosen_rows = ((s_row == row_slot[0]) | (s_row == row_slot[1])).astype(BF)
    s_lane = iota((32, 128), 1)
    picks = [(s_lane == col_slot[k]).astype(BF) for k in range(2)]
    out_at, in_at = iota((128, 128), 0), iota((128, 128), 1)
    turn = (
        in_at == ((out_at // 2) % 8) * 16 + (out_at // 16) * 2 + out_at % 2
    ).astype(BF)

    for s in o_sends:
        s.wait_recv()
    lse = [jnp.transpose(st_out[0])] + [jnp.transpose(st_in[dy]) for dy in range(1, NY)]
    top = jnp.maximum(jnp.maximum(lse[0], lse[1]), jnp.maximum(lse[2], lse[3]))
    weights = [jnp.exp2(t - top) for t in lse]
    inv = 1.0 / (weights[0] + weights[1] + weights[2] + weights[3])
    sum_a = jnp.zeros((256, 128), F32)
    sum_b = jnp.zeros((256, 128), F32)
    for dy in range(NY):
        part = (o_out[0] if dy == 0 else o_in[dy]).astype(F32)
        share = weights[dy] * inv
        sum_a = sum_a + part[:, :128] * share[:, 0:1]
        sum_b = sum_b + part[:, 128:] * jnp.where(lane < 64, share[:, 1:2], share[:, 2:3])
    mg[:, :128] = sum_a.astype(BF)
    mg[:, 128:] = sum_b.astype(BF)
    swap = send(mg.at[pl.ds(high, 128)], mg_in, gs, gr, z, y, mate, x)
    swap.start()
    all_sends.append(swap)
    for load in loads[4:8]:
        load.wait()
    swap.wait_recv()
    pj[...] = (dot(mg[core_rows], wo[0]) + dot(mg_in[...], wo[1])).astype(BF)

    def rows_to(d, at, count):
        return pl.ds(pl.multiple_of(xp(d) * ROWS + at, 16), count)

    def both(a, b):
        return (a.astype(F32) + b.astype(F32)).astype(BF)

    first_up = send(pj.at[rows_to(2, 0, 16)], pj_half.at[0], ps.at[0], pr.at[0], z, y, c, up)
    first_down = send(pj.at[rows_to(2, 16, 16)], pj_half.at[1], ps.at[1], pr.at[1], z, y, c, down)
    then_up = send(pj.at[rows_to(1, 0, 32)], pj_in.at[0], ps.at[2], pr.at[2], z, y, c, up)
    then_down = send(pj.at[rows_to(-1, 0, 32)], pj_in.at[1], ps.at[3], pr.at[3], z, y, c, down)
    first_up.start()
    first_down.start()
    first_up.wait_recv()
    pj[rows_to(1, 0, 16)] = both(pj[rows_to(1, 0, 16)], pj_half[0])
    then_up.start()
    first_down.wait_recv()
    pj[rows_to(-1, 16, 16)] = both(pj[rows_to(-1, 16, 16)], pj_half[1])
    then_down.start()
    all_sends += [first_up, first_down, then_up, then_down]
    total = res[...].astype(F32) + pj[rows_to(0, 0, 32)].astype(F32)
    then_up.wait_recv()
    then_down.wait_recv()
    total = total + pj_in[0].astype(F32) + pj_in[1].astype(F32)
    hidden = total.astype(BF)
    res[...] = hidden
    v = hidden.astype(F32)
    v = v * lax.rsqrt(jnp.mean(v * v, axis=1, keepdims=True) + EPSILON)
    normed = (v * fg[...]).astype(BF)

    blocks = [(dy, dc) for dy in range(NY) for dc in range(2)]
    z_order = (4, 3, 5, 2, 6, 1, 7)
    b_order = (4, 5, 2, 3, 6, 7, 1)

    def b16(i):
        return pl.ds(i * 16, 16)

    dz = [[None] * 8 for _ in range(CHUNKS)]
    dy_ = [[None] * 8 for _ in range(CHUNKS)]
    dx = [None] * CHUNKS
    for j in range(CHUNKS):
        for d in range(1, 8):
            dz[j][d] = send(
                disp.at[j, b16(d)], z_in.at[j, b16(d)], dzs.at[j, d], dzr.at[j, d], zp(d), y, c, x
            )
            py, pc = blocks[d]
            dy_[j][d] = send(
                y_out.at[j, b16(d)], x_in.at[j, 0, b16(d)], dys.at[j, d], dyr.at[j, d],
                z, yp(py), (c + pc) % 2, x,
            )
        top_half, low_half = pl.ds(0, 64), pl.ds(64, 64)
        dx[j] = (
            send(x_in.at[j, 0], x_in.at[j, 1], dxs.at[j, 0], dxr.at[j, 0], z, y, c, up),
            send(x_in.at[j, 0], x_in.at[j, 3], dxs.at[j, 1], dxr.at[j, 1], z, y, c, down),
            send(
                x_in.at[j, 1, top_half], x_in.at[j, 2, top_half],
                dxs.at[j, 2], dxr.at[j, 2], z, y, c, up,
            ),
            send(
                x_in.at[j, 3, low_half], x_in.at[j, 2, low_half],
                dxs.at[j, 3], dxr.at[j, 3], z, y, c, down,
            ),
        )
        all_sends += dz[j][1:] + dy_[j][1:] + list(dx[j])

    for j in range(CHUNKS):
        disp[j] = dot(chosen_rows, normed[:, j * WIDE : (j + 1) * WIDE]).astype(BF)
        for d in z_order:
            dz[j][d].start()
        z_in[j, :16] = disp[j, :16]

    for t in range(CHUNKS + 2):
        if t < CHUNKS:
            for d in z_order:
                dz[t][d].wait_recv()
            y_out[t] = dot(turn, z_in[t]).astype(BF)
            for d in b_order:
                dy_[t][d].start()
            x_in[t, 0, :16] = y_out[t, :16]
        if 1 <= t <= CHUNKS:
            j = t - 1
            for d in b_order:
                dy_[j][d].wait_recv()
            dx[j][0].start()
            dx[j][1].start()
        if t == 2:
            loads[8].wait()
            loads[9].wait()
        if t >= 2:
            j = t - 2
            dx[j][0].wait_recv()
            dx[j][2].start()
            dx[j][1].wait_recv()
            dx[j][3].start()
            dx[j][2].wait_recv()
            dx[j][3].wait_recv()
            arrived = x_in[j].reshape(512, WIDE)
            g = dot(arrived, wg[j * WIDE : (j + 1) * WIDE])
            u = dot(arrived, wu[j * WIDE : (j + 1) * WIDE])
            if j == 0:
                acc_g[...] = g
                acc_u[...] = u
            elif j < CHUNKS - 1:
                acc_g[...] += g
                acc_u[...] += u
            else:
                g = acc_g[...] + g
                act[...] = (g / (1.0 + jnp.exp(-g)) * (acc_u[...] + u)).astype(BF)

    rx = [None] * CHUNKS
    ry = [[None] * 8 for _ in range(CHUNKS)]
    rz = [[None] * 8 for _ in range(CHUNKS)]
    for j in range(CHUNKS):
        rx[j] = (
            send(p_out.at[j, 2, pl.ds(0, 64)], p_half.at[j, 0], rxs.at[j, 0], rxr.at[j, 0], z, y, c, up),
            send(p_out.at[j, 2, pl.ds(64, 64)], p_half.at[j, 1], rxs.at[j, 1], rxr.at[j, 1], z, y, c, down),
            send(p_out.at[j, 3], p_in.at[j, 0], rxs.at[j, 2], rxr.at[j, 2], z, y, c, up),
            send(p_out.at[j, 1], p_in.at[j, 1], rxs.at[j, 3], rxr.at[j, 3], z, y, c, down),
        )
        for d in range(1, 8):
            py, pc = blocks[d]
            ry[j][d] = send(
                r_sum.at[j, b16(d)], ry_in.at[j, b16(d)], rys.at[j, d], ryr.at[j, d],
                z, yp(-py), (c + pc) % 2, x,
            )
            rz[j][d] = send(
                rz_out.at[j, b16(d)], rz_in.at[j, b16(d)], rzs.at[j, d], rzr.at[j, d],
                zp(-d), y, c, x,
            )
        all_sends += list(rx[j]) + ry[j][1:] + rz[j][1:]

    loads[10].wait()
    for t in range(CHUNKS + 4):
        if t < CHUNKS:
            part = dot(act[...], wd[:, t * WIDE : (t + 1) * WIDE]).astype(BF)
            p_out[t] = part.reshape(4, 128, WIDE)
            rx[t][0].start()
            rx[t][1].start()
        if 1 <= t <= CHUNKS:
            j = t - 1
            rx[j][0].wait_recv()
            p_out[j, 3, :64] = both(p_out[j, 3, :64], p_half[j, 0])
            rx[j][2].start()
            rx[j][1].wait_recv()
            p_out[j, 1, 64:] = both(p_out[j, 1, 64:], p_half[j, 1])
            rx[j][3].start()
        if 2 <= t <= CHUNKS + 1:
            j = t - 2
            rx[j][2].wait_recv()
            rx[j][3].wait_recv()
            total = p_out[j, 0].astype(F32) + p_in[j, 0].astype(F32) + p_in[j, 1].astype(F32)
            r_sum[j] = total.astype(BF)
            for d in b_order:
                ry[j][d].start()
            ry_in[j, :16] = r_sum[j, :16]
        if 3 <= t <= CHUNKS + 2:
            j = t - 3
            for d in b_order:
                ry[j][d].wait_recv()
            rz_out[j] = dot(turn, ry_in[j]).astype(BF)
            for d in z_order:
                rz[j][d].start()
            rz_in[j, :16] = rz_out[j, :16]
        if t >= 4:
            j = t - 4
            for d in z_order:
                rz[j][d].wait_recv()
            back = rz_in[j]
            mixed = col_w[0] * dot(picks[0], back) + col_w[1] * dot(picks[1], back)
            cols = slice(j * WIDE, (j + 1) * WIDE)
            out_ref[:, cols] = (res[:, cols].astype(F32) + mixed).astype(BF)

    for s in all_sends:
        s.wait_send()


def body(
    query_a, query_b, latent, rope_key, latent_gain, key_a_weight, value_a_weight, key_b_weight,
    value_b_weight, out_a_weight, out_b_weight, residual, ffn_gain, routes, route_weight,
    expert_gate, expert_up, expert_down,
):
    hbm = pl.BlockSpec(memory_space=pltpu.HBM)
    dma = pltpu.SemaphoreType.DMA
    vm = pltpu.VMEM
    ta, tb = angle_tables()
    return pl.pallas_call(
        layer_kernel,
        out_shape=jax.ShapeDtypeStruct(residual.shape, BF),
        in_specs=[hbm] * 20,
        out_specs=pl.BlockSpec(memory_space=pltpu.VMEM),
        scratch_shapes=[
            vm((128, 384), BF), vm((128, 512), BF), vm((32, 512), BF), vm((32, 64), BF),
            vm((1, 512), F32), vm((32, 2048), BF), vm((1, 2048), F32),
            vm((2, 32), jnp.int32), vm((2, 32), F32), vm((64, 256), F32), vm((128, 256), F32),
            vm((32, 640), BF), vm((2, 128, 512), BF), vm((8, 256, 640), BF), vm((4, 256, 512), BF),
            vm((512, 512), BF), vm((2, 256, 2048), BF),
            vm((8, 256, 256), BF), vm((8, 256, 128), BF), vm((8, 256, 128), BF),
            vm((8, 256, 256), BF), vm((3, 8, 256, 256), F32),
            vm((4, 256, 256), BF), vm((4, 256, 256), BF), vm((4, 8, 256), F32), vm((4, 8, 256), F32),
            vm((256, 256), BF), vm((128, 256), BF), vm((128, 2048), BF),
            vm((2, 16, 2048), BF), vm((2, 32, 2048), BF),
            vm((2048, 768), BF), vm((2048, 768), BF), vm((768, 2048), BF),
            vm((CHUNKS, 128, WIDE), BF), vm((CHUNKS, 128, WIDE), BF), vm((CHUNKS, 128, WIDE), BF),
            vm((CHUNKS, 4, 128, WIDE), BF), vm((512, 768), F32), vm((512, 768), F32),
            vm((512, 768), BF), vm((CHUNKS, 4, 128, WIDE), BF), vm((CHUNKS, 2, 64, WIDE), BF),
            vm((CHUNKS, 2, 128, WIDE), BF), vm((CHUNKS, 128, WIDE), BF),
            vm((CHUNKS, 128, WIDE), BF), vm((CHUNKS, 128, WIDE), BF), vm((CHUNKS, 128, WIDE), BF),
            dma((11,)), dma((11,)),
            dma((8,)), dma((8,)), dma((8, 4)), dma((8, 4)), dma((8,)), dma((8,)),
            dma((2, 5)), dma((2, 5)), dma((4,)), dma((4,)), dma((4,)), dma((4,)), dma, dma,
            dma((4,)), dma((4,)),
            dma((CHUNKS, 8)), dma((CHUNKS, 8)), dma((CHUNKS, 8)), dma((CHUNKS, 8)),
            dma((CHUNKS, 4)), dma((CHUNKS, 4)), dma((CHUNKS, 4)), dma((CHUNKS, 4)),
            dma((CHUNKS, 8)), dma((CHUNKS, 8)), dma((CHUNKS, 8)), dma((CHUNKS, 8)),
        ],
        compiler_params=pltpu.CompilerParams(
            collective_id=0, has_side_effects=True, vmem_limit_bytes=67043328
        ),
        cost_estimate=pl.CostEstimate(
            flops=2 * 10**10, bytes_accessed=2 * 10**7, transcendentals=10**7
        ),
    )(
        query_a, query_b, latent, rope_key, latent_gain.reshape(1, -1), key_a_weight,
        value_a_weight, key_b_weight, value_b_weight, out_a_weight, out_b_weight, residual,
        ffn_gain.reshape(1, -1), routes.T, route_weight.T, expert_gate, expert_up, expert_down,
        jnp.asarray(ta), jnp.asarray(tb),
    )


def solution(mesh):
    placed = (
        P("sp", "tp"),
        P("sp", "tp"),
        P(("sp", "tp"), None),
        P(("sp", "tp"), None),
        P(),
        P(None, "tp"),
        P(None, "tp"),
        P(None, "tp"),
        P(None, "tp"),
        P("tp", None),
        P("tp", None),
        P(("sp", "tp"), None),
        P(),
        P(("sp", "tp"), None),
        P(("sp", "tp"), None),
        P("sp", None, "tp"),
        P("sp", None, "tp"),
        P("sp", "tp", None),
    )
    return jax.shard_map(
        body, mesh=mesh, in_specs=placed, out_specs=P(("sp", "tp"), None), check_vma=False
    )
```

time: 264 us -> 149 us (0.56)
  Pallas kernels: 56.1 us -> 147 us
  waiting for transfers between devices: 79.2 us -> 0 us
  local copies, waits for them, and re-layouts: 37.9 us -> 1.57 us
  blocking collectives: 35.7 us -> 0 us
  matrix products: 19.3 us -> 0 us
  between operations: 13.6 us -> 0.01 us
  starting transfers between devices: 11 us -> 0 us
  other arithmetic: 9.81 us -> 0 us
    pallas_call x1, Pallas kernels: 56.1 us -> 147 us  [body(): pl.pallas_call(layer_kernel, out_shape=jax.ShapeDtypeStruct(residual.shap...]
    all_to_all x1 -> x0, blocking collectives: 35.7 us -> none  [body(): lax.all_to_all(outgoing, 'sp', split_axis=0, concat_axis=0, tiled=True)]
    reduce_scatter x1 -> x0, waiting for transfers between devices: 32.6 us -> none  [body(): lax.psum_scatter(partials.astype(jnp.bfloat16), 'tp', scatter_dimension=1...]
    all_gather x1 -> x0, waiting for transfers between devices: 29.1 us -> none  [body(): lax.all_gather(lax.all_to_all(outgoing, 'sp', split_axis=0, concat_axis=0...]
    dot_general x5 -> x0, matrix products: 19.3 us -> none  [the longest x1 8.71 us: body(): jnp.dot(hidden, expert_down[0], preferred_element_type=jnp.float32)]
    unnamed x41 -> x1, local copies, waits for them, and re-layouts: 20.5 us -> 1.57 us
    all_to_all x1 -> x0, waiting for transfers between devices: 17.6 us -> none  [body(): lax.all_to_all(summed, 'sp', split_axis=0, concat_axis=0, tiled=True)]
    all_to_all x1 -> x0, starting transfers between devices: 10.9 us -> none  [body(): lax.all_to_all(summed, 'sp', split_axis=0, concat_axis=0, tiled=True)]
  transfers between devices with their start and end apart: 3 -> 0, of which waited for: 3 -> 0; matrix products, arithmetic and copies ran while one was open for 0% -> 0% of each run, Pallas kernels for 0% -> 0%
where the time goes in v1:
time: 149 us
  Pallas kernels  147 us (99%)
  local copies, waits for them, and re-layouts  1.57 us (1%)
    pallas_call x1, Pallas kernels, body(): pl.pallas_call(layer_kernel, out_shape=jax.ShapeDtypeStruct(residual.shap...  147 us

profile of v1, /device:TPU:1, one launch (start us, length us, event | category | flops | bytes accessed | tf_op | source)
XLA Modules:
  0.0 149.0 jit_solution(15320776613233394186)
XLA Ops:
  0.0 147.4 %shard_map.190 = bf16[32,2048]{1,0:T(8,128)(2,1)} custom-call(bf16[128,384]{1,0:T(8,128)(2,1)} %qa_ref.1, bf16[128,512]{1,0:T(8,128)(2,1)} %qb_ref.1, bf16[32,512]{1,0:T(8,128)(2,1)} %lat_ref.1, bf16[32,64]{1,0:T(8,128)(2,1)} %rope_ref.1, f32[1,512]{1,0:T(1,128)} %bitcast.5, bf16[512,256]{1,0:T(8,128)(2,1)} %ka_ref.1, bf16[512,256]{1,0:T(8,128)(2,1)} %va_ref.1, ...), custom_call_target="tpu_custom_call" | custom-call | flops 20000000000 | bytes 20000000 | tf_op jit(solution)/shard_map/pallas_call | solution.py:600
  147.5 1.6 %copy.22 = bf16[32,2048]{1,0:T(8,128)(2,1)} copy(bf16[32,2048]{1,0:T(8,128)(2,1)} %shard_map.190) | data formatting | bytes 262144

commit v2 on v1

v2 whole, which is shorter than its diff:
```python
import functools

import jax
import jax.numpy as jnp
import numpy as np
from jax import lax
from jax.experimental import pallas as pl
from jax.experimental.pallas import tpu as pltpu
from jax.sharding import PartitionSpec as P

NZ, NY, NX = 8, 4, 4
TOKENS_PER_SP = 128
ROWS = 32
OUT = ((0, 512), (512, 512), (1024, 512), (None, 128), (1536, 512))
BACK = ((0, 512), (512, 512), (1024, 512), (1536, 256), (1792, 256))
LOG2E = 1.4426950408889634
EPSILON = 1e-06
BASE_THETA = 500000.0
MASKED = -1e30
MESH_ID = pl.DeviceIdType.MESH
BF, F32 = jnp.bfloat16, jnp.float32


def angle_tables():
    inverse = BASE_THETA ** (-np.arange(0, 64, 2, dtype=np.float64) / 64)
    lanes = np.tile(inverse, 4)[None, :]

    def table(positions):
        angles = positions[:, None] * lanes
        return np.concatenate([np.cos(angles), np.sin(angles)], axis=1).astype(np.float32)

    return table(np.arange(64) * 128.0), table(np.arange(128) * 1.0)


def send(src, dst, send_sem, recv_sem, z, y, c, x):
    return pltpu.make_async_remote_copy(
        src_ref=src,
        dst_ref=dst,
        send_sem=send_sem,
        recv_sem=recv_sem,
        device_id=(z * 8 + y * 2 + c, x),
        device_id_type=MESH_ID,
    )


def dot(a, b):
    return jnp.dot(a, b, preferred_element_type=F32)


def nt_dot(a, b):
    return lax.dot_general(a, b, (((1,), (1,)), ((), ())), preferred_element_type=F32)


def iota(shape, dim):
    return lax.broadcasted_iota(jnp.int32, shape, dim)


def layer_kernel(
    qa_ref, qb_ref, lat_ref, rope_ref, gain_ref, ka_ref, va_ref, kb_ref, vb_ref, oa_ref, ob_ref,
    res_ref, fg_ref, rt_ref, wt_ref, eg_ref, eu_ref, ed_ref, ta_ref, tb_ref,
    out_ref,
    qa, qb, lat, rope, gain, res, fg, rt, wt, ta, tb,
    lat_own, q_own, latg, qg, w, wo, k_a, k_b0, k_b1, val, o_out, o_in, st_out, st_in,
    tops, sums, mixes, pj, pj_in,
    wg, wu, wd, disp, z_in, y_out, x_in, acc_g, acc_u, act, p_out, p_half, p_in, r_sum, ry_in,
    rz_out, rz_in,
    in_sem, w_sem, zs, zr, xs, xr, ms, mr, qs, qr, os_, or_, ss, sr, ps, pr,
    dzs, dzr, dys, dyr, dxs, dxr, rxs, rxr, rys, ryr, rzs, rzr,
):
    sp = lax.axis_index("sp")
    x = lax.axis_index("tp")
    z, y, c = sp // 8, (sp // 2) % 4, sp % 2
    mate = 1 - c
    low = pl.multiple_of(c * 128, 128)
    high = pl.multiple_of(mate * 128, 128)
    up = (x + 1) % NX
    down = (x + NX - 1) % NX

    def zp(d):
        return (z + d + NZ) % NZ

    def yp(d):
        return (y + d + NY) % NY

    def xp(d):
        return (x + d + NX) % NX

    small = [
        pltpu.make_async_copy(src, dst, in_sem.at[i])
        for i, (src, dst) in enumerate(
            (
                (lat_ref, lat), (rope_ref, rope), (gain_ref, gain), (ta_ref, ta), (tb_ref, tb),
                (qa_ref, qa), (qb_ref, qb), (res_ref, res), (fg_ref, fg), (rt_ref, rt), (wt_ref, wt),
            )
        )
    ]
    for load in small:
        load.start()
    loads = [
        pltpu.make_async_copy(r.at[:, pl.ds(low, 128)], w.at[:, pl.ds(i * 128, 128)], w_sem.at[i])
        for i, r in enumerate((ka_ref, kb_ref, va_ref, vb_ref))
    ]
    for i, at in enumerate((low, high)):
        for j, r in enumerate((oa_ref, ob_ref)):
            loads.append(
                pltpu.make_async_copy(
                    r.at[pl.ds(at, 128), :], wo.at[i, pl.ds(j * 128, 128)], w_sem.at[4 + 2 * i + j]
                )
            )
    for i, (src, dst) in enumerate(((eg_ref, wg), (eu_ref, wu), (ed_ref, wd))):
        loads.append(pltpu.make_async_copy(src.at[0], dst, w_sem.at[8 + i]))
    for load in loads:
        load.start()

    barrier = pltpu.get_barrier_semaphore()

    def greet(pz, py, pc, px):
        pl.semaphore_signal(
            barrier, inc=1, device_id=(pz * 8 + py * 2 + pc, px), device_id_type=MESH_ID
        )

    for d in range(1, NZ):
        greet(zp(d), y, c, x)
    for d in range(1, NX):
        greet(z, y, c, xp(d))
    for dy in range(NY):
        for dc in range(2):
            if dy or dc:
                greet(z, yp(dy), (c + dc) % 2, x)

    for load in small[:5]:
        load.wait()
    v = lat[...].astype(F32)
    v = v * lax.rsqrt(jnp.mean(v * v, axis=1, keepdims=True) + EPSILON)
    lat_own[:, :512] = (v * gain[...]).astype(BF)
    base = jnp.sum(jnp.where(iota((64, 256), 0) == sp, ta[...], 0.0), axis=0, keepdims=True)
    cos_a, sin_a = base[:, :128], base[:, 128:]

    def turning(cos_b, sin_b):
        lane = iota(cos_b.shape, 1)
        sine = sin_a * cos_b + cos_a * sin_b
        return cos_a * cos_b - sin_a * sin_b, jnp.where(lane % 64 < 32, -sine, sine)

    def rotated(tile, cosine, sine):
        lane = iota(tile.shape, 1)
        other = jnp.where(
            lane % 64 < 32, pltpu.roll(tile, 96, axis=1), pltpu.roll(tile, 32, axis=1)
        )
        return tile * cosine + other * sine

    own_32 = pl.ds(pl.multiple_of(x * ROWS, ROWS), ROWS)
    cosine, sine = turning(tb[own_32, :128], tb[own_32, 128:])
    twice = (iota((64, 128), 1) % 64 == iota((64, 128), 0)).astype(BF)
    lat_own[:, 512:] = rotated(dot(rope[...], twice), cosine, sine).astype(BF)

    pl.semaphore_wait(barrier, NZ - 1 + NX - 1 + 2 * NY - 1)

    def rows_of(px, at, count):
        return pl.ds(pl.multiple_of(c * 128 + px * ROWS + at, 16), count)

    core_rows = pl.ds(low, 128)
    all_sends = []

    z_sends = [None] + [
        send(lat_own, latg.at[d, rows_of(x, 0, 32)], zs.at[d], zr.at[d], zp(d), y, c, x)
        for d in range(1, NZ)
    ]
    all_sends += z_sends[1:]

    def ring(d):
        own = lat_own if d == 0 else latg.at[d, rows_of(x, 0, 32)]
        to = latg.at[d, rows_of(x, 0, 32)]
        one = latg.at[d, rows_of(down, 0, 16)]
        two = latg.at[d, rows_of(up, 16, 16)]
        return (
            send(own, to, xs.at[d, 0], xr.at[d, 0], z, y, c, up),
            send(own, to, xs.at[d, 1], xr.at[d, 1], z, y, c, down),
            send(one, one, xs.at[d, 2], xr.at[d, 2], z, y, c, up),
            send(two, two, xs.at[d, 3], xr.at[d, 3], z, y, c, down),
        )

    x_sends = [ring(d) for d in range(NZ)]
    for d in range(NZ):
        all_sends += x_sends[d]
    x_sends[0][0].start()
    x_sends[0][1].start()
    for d in (1, 7, 2, 6, 3, 5, 4):
        z_sends[d].start()
    latg[0, rows_of(x, 0, 32)] = lat_own[...]

    small[5].wait()
    small[6].wait()
    cosine, sine = turning(tb[:, :128], tb[:, 128:])
    lane = iota((128, 128), 1)
    t1 = qa[:, 128:256]
    t2 = qa[:, 256:384]
    r1 = rotated(t1.astype(F32), cosine, sine)
    r2 = rotated(t2.astype(F32), cosine, sine)
    mixed = jnp.where(lane < 64, t2.astype(F32), t1.astype(F32))
    q_own[0, :, :128] = qa[:, :128]
    q_own[0, :, 128:256] = jnp.where(lane < 64, r1, 0.0).astype(BF)
    q_own[1, :, :128] = pltpu.roll(mixed, 64, axis=1).astype(BF)
    q_own[1, :, 128:256] = jnp.where(lane < 64, 0.0, r2).astype(BF)
    for h in range(4):
        t = qb[:, h * 128 : h * 128 + 128].astype(F32)
        t = jnp.where(lane < 64, t, rotated(t, cosine, sine))
        if h % 2:
            t = pltpu.roll(t, 64, axis=1)
        q_own[h // 2, :, 256 + (h % 2) * 128 : 384 + (h % 2) * 128] = t.astype(BF)

    q_sends = []
    for dc in range(2):
        pc = (c + dc) % 2
        there = pl.ds(pl.multiple_of(pc * 128, 128), 128)
        one = qg.at[1, pl.ds(pl.multiple_of(pc * 128, 64), 64)]
        one_to = qg.at[2, pl.ds(pl.multiple_of(pc * 128, 64), 64)]
        two = qg.at[3, pl.ds(pl.multiple_of(pc * 128 + 64, 64), 64)]
        two_to = qg.at[2, pl.ds(pl.multiple_of(pc * 128 + 64, 64), 64)]
        q_sends.append(
            (
                send(q_own.at[pc], qg.at[1, core_rows], qs.at[dc, 0], qr.at[dc, 0], z, yp(1), pc, x),
                send(q_own.at[pc], qg.at[3, core_rows], qs.at[dc, 1], qr.at[dc, 1], z, yp(-1), pc, x),
                send(one, one_to, qs.at[dc, 2], qr.at[dc, 2], z, yp(1), c, x),
                send(two, two_to, qs.at[dc, 3], qr.at[dc, 3], z, yp(-1), c, x),
            )
        )
    q_mate = send(q_own.at[mate], qg.at[0, core_rows], qs.at[0, 4], qr.at[0, 4], z, y, mate, x)
    all_sends += q_sends[0] + q_sends[1] + (q_mate,)
    for dc in range(2):
        q_sends[dc][0].start()
        q_sends[dc][1].start()
    q_mate.start()
    qg[0, core_rows] = q_own[c]

    m_sends = [
        send(latg.at[d, core_rows], latg.at[d, core_rows], ms.at[d], mr.at[d], z, y, mate, x)
        for d in range(NZ)
    ]
    all_sends += m_sends

    def forward(d):
        x_sends[d][0].wait_recv()
        x_sends[d][2].start()
        x_sends[d][1].wait_recv()
        x_sends[d][3].start()

    def to_mate(d):
        x_sends[d][2].wait_recv()
        x_sends[d][3].wait_recv()
        m_sends[d].start()

    for load in small[7:]:
        load.wait()
    eye = iota((32, 32), 0) == iota((32, 32), 1)
    before = iota((32, 32), 1) < iota((32, 32), 0)
    after = iota((32, 32), 0) < iota((32, 32), 1)
    chosen = rt[...]
    row_e = [chosen[k : k + 1].astype(F32) for k in range(2)]
    col_e = [jnp.sum(jnp.where(eye, e, 0.0), axis=1, keepdims=True) for e in row_e]
    share = wt[...]
    col_w = [
        jnp.sum(jnp.where(eye, share[k : k + 1], 0.0), axis=1, keepdims=True) for k in range(2)
    ]

    def slot(e, rank):
        e = e.astype(jnp.int32)
        dz = (e // 8 - z + NZ) % NZ
        dy = ((e // 2) % 4 - y + NY) % NY
        dc = (e % 2 - c + 2) % 2
        return dz * 16 + dy * 4 + dc * 2 + rank.astype(jnp.int32)

    row_slot, col_slot = [], []
    for k in range(2):
        rank_row = jnp.zeros((1, 32), F32)
        rank_col = jnp.zeros((32, 1), F32)
        for o in range(2):
            same = (col_e[o] == row_e[k]) & after
            rank_row = rank_row + jnp.sum(jnp.where(same, 1.0, 0.0), axis=0, keepdims=True)
            same = (row_e[o] == col_e[k]) & before
            rank_col = rank_col + jnp.sum(jnp.where(same, 1.0, 0.0), axis=1, keepdims=True)
        row_slot.append(slot(row_e[k], rank_row))
        col_slot.append(slot(col_e[k], rank_col))
    s_row = iota((128, 32), 0)
    chosen_rows = ((s_row == row_slot[0]) | (s_row == row_slot[1])).astype(BF)
    s_lane = iota((32, 128), 1)
    picks = [(s_lane == col_slot[k]).astype(BF) for k in range(2)]
    out_at, in_at = iota((128, 128), 0), iota((128, 128), 1)
    turn = (
        in_at == ((out_at // 2) % 8) * 16 + (out_at // 16) * 2 + out_at % 2
    ).astype(BF)

    lane = iota((256, 128), 1)
    lane_512 = iota((512, 128), 1)
    row = iota((512, 128), 0)
    col = iota((512, 128), 1)
    factors = (LOG2E * 192**-0.5, LOG2E * 128**-0.5, LOG2E * 128**-0.5)

    def expand(i, d):
        at = slice(i * 256, i * 256 + 256)
        block = latg[d]
        made = dot(block[:, :512], w[...]).astype(BF)
        turned = block[:, 512:]
        b = made[:, 128:256]
        k_a[at, :128] = made[:, :128]
        k_a[at, 128:] = turned
        k_b0[at] = jnp.where(lane < 64, b, turned)
        k_b1[at] = jnp.where(lane < 64, turned, b)
        val[at] = made[:, 256:]

    def attend(i, ds):
        count = 256 * len(ds)
        q = qg[pl.ds(i * 2, 2)].reshape(512, 512)

        def raw(h):
            if h == 0:
                return nt_dot(q[:, :256], k_a[:count])
            if h == 1:
                return nt_dot(q[:, 256:384], k_b0[:count])
            return nt_dot(q[:, 384:], k_b1[:count])

        later = raw(0)
        for h in range(3):
            s = later
            if h < 2:
                later = raw(h + 1)
            tiles = [s[:, t : t + 128] for t in range(0, count, 128)]
            if ds[0] == 0:
                first, second = (yp(-2 * i) - y) * 256, (yp(-2 * i - 1) - y) * 256 - 256
                last = row + jnp.where(row < 256, first, second)
                for t in range(2):
                    tiles[t] = jnp.where(last >= col + t * 128, tiles[t], MASKED)
            if len(ds) == 2:
                for t in range(2, 4):
                    tiles[t] = jnp.where(z >= ds[1], tiles[t], MASKED)
            top = functools.reduce(jnp.maximum, tiles)
            top = jnp.broadcast_to(jnp.max(top, axis=1, keepdims=True), (512, 128))
            if ds[0]:
                old = tops[i, h]
                top = jnp.maximum(top, old)
            tops[i, h] = top
            tiles = [jnp.exp2((t - top) * factors[h]) for t in tiles]
            total = functools.reduce(jnp.add, tiles)
            weights = jnp.concatenate([t.astype(BF) for t in tiles], axis=1)
            product = dot(weights, val[:count, :128] if h == 0 else val[:count, 128:])
            if ds[0]:
                kept = jnp.exp2((old - top) * factors[h])
                sums[i, h] = sums[i, h] * kept + total
                mixes[i, h] = mixes[i, h] * kept + product
            else:
                sums[i, h] = total
                mixes[i, h] = product

    def finish(i):
        outs, lses = [], []
        for h in range(3):
            total = jnp.sum(sums[i, h], axis=1, keepdims=True)
            outs.append(mixes[i, h] / total)
            lses.append(tops[i, h] * factors[h] + jnp.log2(total))
        mixed = jnp.where(lane_512 < 64, outs[1], outs[2])
        o_out[pl.ds(2 * i, 2), :, :128] = outs[0].astype(BF).reshape(2, 256, 128)
        o_out[pl.ds(2 * i, 2), :, 128:] = mixed.astype(BF).reshape(2, 256, 128)
        stats = jnp.where(lane_512 == 0, lses[0], jnp.where(lane_512 == 1, lses[1], lses[2]))
        st_out[i] = jnp.transpose(stats)[:8]

    def arrived_z(d):
        z_sends[d].wait_recv()
        x_sends[d][0].start()
        x_sends[d][1].start()

    def forward_q(dc):
        q_sends[dc][0].wait_recv()
        q_sends[dc][2].start()
        q_sends[dc][1].wait_recv()
        q_sends[dc][3].start()

    arrived_z(1)
    arrived_z(7)
    forward(0)
    arrived_z(2)
    forward(1)
    to_mate(0)
    forward_q(0)
    arrived_z(6)
    forward(7)
    to_mate(1)
    forward_q(1)
    arrived_z(3)
    forward(2)
    to_mate(7)
    arrived_z(5)
    forward(6)
    to_mate(2)
    arrived_z(4)
    forward(3)
    to_mate(6)
    forward(5)
    forward(4)
    for load in loads[:4]:
        load.wait()
    q_mate.wait_recv()
    for dc in range(2):
        q_sends[dc][2].wait_recv()
        q_sends[dc][3].wait_recv()
    for i, d in enumerate((0, 1, 2, 7)):
        m_sends[d].wait_recv()
        if d < 2:
            expand(i, d)
        else:
            pl.when(z >= d)(functools.partial(expand, i, d))

    def near(i, carried):
        pl.when(z < 2)(functools.partial(attend, i, (0, 1)))
        pl.when((z >= 2) & (z < 7))(functools.partial(attend, i, (0, 1, 2)))
        pl.when(z == 7)(functools.partial(attend, i, (0, 1, 2, 7)))

        @pl.when(i == 0)
        def _():
            to_mate(3)
            to_mate(5)
            to_mate(4)

        return carried

    lax.fori_loop(0, 2, near, 0)

    places = [(dy, dc) for dy in range(NY) for dc in range(2)]
    o_sends = [None] * 8
    st_sends = [None] * 8
    for k in range(1, 8):
        dy, dc = places[k]
        pc = (c + dc) % 2
        at = pl.multiple_of(pc * 128, 128)
        o_sends[k] = send(
            o_out.at[dy, pl.ds(at, 128)], o_in.at[k], os_.at[k], or_.at[k], z, yp(-dy), pc, x
        )
        st_sends[k] = send(
            st_out.at[dy // 2, :, pl.ds(pl.multiple_of((dy % 2) * 256 + at, 128), 128)],
            st_in.at[k], ss.at[k], sr.at[k], z, yp(-dy), pc, x,
        )
    all_sends += o_sends[1:] + st_sends[1:]

    for i, d in enumerate((3, 4, 5, 6)):
        m_sends[d].wait_recv()
        pl.when(z >= (3 if d == 4 else d))(functools.partial(expand, i, d))

    def far(t, carried):
        i = 1 - t
        pl.when((z == 3) | (z == 4))(functools.partial(attend, i, (3, 4)))
        pl.when(z == 5)(functools.partial(attend, i, (3, 4, 5)))
        pl.when(z >= 6)(functools.partial(attend, i, (3, 4, 5, 6)))
        finish(i)

        @pl.when(t == 0)
        def _():
            for k in (4, 5, 6, 7):
                o_sends[k].start()
                st_sends[k].start()

        return carried

    lax.fori_loop(0, 2, far, 0)
    for k in (2, 3, 1):
        o_sends[k].start()
        st_sends[k].start()
    for load in loads[4:8]:
        load.wait()
    for k in range(1, 8):
        o_sends[k].wait_recv()
        st_sends[k].wait_recv()

    lane = iota((128, 128), 1)
    made = []
    for dc in range(2):
        parts, lse = [], []
        for dy in range(NY):
            k = dy * 2 + dc
            parts.append(o_out[0, core_rows] if k == 0 else o_in[k])
            lse.append(jnp.transpose(st_out[0, :, core_rows] if k == 0 else st_in[k]))
        top = jnp.maximum(jnp.maximum(lse[0], lse[1]), jnp.maximum(lse[2], lse[3]))
        weights = [jnp.exp2(t - top) for t in lse]
        inv = 1.0 / (weights[0] + weights[1] + weights[2] + weights[3])
        sum_a = jnp.zeros((128, 128), F32)
        sum_b = jnp.zeros((128, 128), F32)
        for dy in range(NY):
            part = parts[dy].astype(F32)
            share = weights[dy] * inv
            sum_a = sum_a + part[:, :128] * share[:, 0:1]
            sum_b = sum_b + part[:, 128:] * jnp.where(lane < 64, share[:, 1:2], share[:, 2:3])
        joined = jnp.concatenate([sum_a.astype(BF), sum_b.astype(BF)], axis=1)
        made.append(joined)

    def rows_to(d):
        return pl.ds(pl.multiple_of(xp(d) * ROWS, ROWS), ROWS)

    def both(a, b):
        return (a.astype(F32) + b.astype(F32)).astype(BF)

    p_sends = []
    for j in range(4):
        cols = slice(j * 512, j * 512 + 512)
        pj[j] = (dot(made[0], wo[0, :, cols]) + dot(made[1], wo[1, :, cols])).astype(BF)
        p_sends.append(
            [
                send(pj.at[j, rows_to(d)], pj_in.at[j, d], ps.at[j, d], pr.at[j, d], z, y, c, xp(d))
                for d in (2, 1, 3)
            ]
        )
        for s in p_sends[j]:
            s.start()
        all_sends += p_sends[j]

    blocks = [(dy, dc) for dy in range(NY) for dc in range(2)]
    z_order = (4, 3, 5, 2, 6, 1, 7)
    b_order = (4, 5, 2, 3, 6, 7, 1)
    count = len(OUT)

    def b16(i):
        return pl.ds(i * 16, 16)

    dz = [[None] * 8 for _ in range(count)]
    dy_ = [[None] * 8 for _ in range(count)]
    dx = [None] * count
    for j in range(count):
        for d in range(1, 8):
            dz[j][d] = send(
                disp[j].at[b16(d)], z_in[j].at[b16(d)], dzs.at[j, d], dzr.at[j, d], zp(d), y, c, x
            )
            py, pc = blocks[d]
            dy_[j][d] = send(
                y_out[j].at[b16(d)], x_in[j].at[0, b16(d)], dys.at[j, d], dyr.at[j, d],
                z, yp(py), (c + pc) % 2, x,
            )
        top_half, low_half = pl.ds(0, 64), pl.ds(64, 64)
        dx[j] = (
            send(x_in[j].at[0], x_in[j].at[1], dxs.at[j, 0], dxr.at[j, 0], z, y, c, up),
            send(x_in[j].at[0], x_in[j].at[3], dxs.at[j, 1], dxr.at[j, 1], z, y, c, down),
            send(
                x_in[j].at[1, top_half], x_in[j].at[2, top_half],
                dxs.at[j, 2], dxr.at[j, 2], z, y, c, up,
            ),
            send(
                x_in[j].at[3, low_half], x_in[j].at[2, low_half],
                dxs.at[j, 3], dxr.at[j, 3], z, y, c, down,
            ),
        )
        all_sends += dz[j][1:] + dy_[j][1:] + list(dx[j])

    def dispatch(j, rows):
        disp[j][...] = dot(chosen_rows, rows).astype(BF)
        for d in z_order:
            dz[j][d].start()
        z_in[j][:16] = disp[j][:16]

    squares = jnp.zeros((ROWS, 1), F32)
    for j in range(4):
        cols = slice(j * 512, j * 512 + 512)
        total = res[:, cols].astype(F32) + pj[j, rows_to(0)].astype(F32)
        for s in p_sends[j]:
            s.wait_recv()
        for d in range(1, NX):
            total = total + pj_in[j, d].astype(F32)
        hidden = total.astype(BF)
        res[:, cols] = hidden
        total = hidden.astype(F32)
        squares = squares + jnp.sum(total * total, axis=1, keepdims=True)
        if j < 3:
            dispatch(j, hidden)
        else:
            exact = lax.rsqrt(squares * (1.0 / 2048) + EPSILON)
            terms = []
            for _ in range(3):
                terms.append(exact.astype(BF))
                exact = exact - terms[-1].astype(F32)
            lane = iota((ROWS, 128), 1)
            scales = jnp.zeros((ROWS, 128), F32)
            for k in range(3):
                scales = jnp.where(lane == k, terms[k].astype(F32), scales)
            dispatch(3, scales.astype(BF))
            dispatch(4, hidden)

    def expert_in(j):
        at, width = OUT[j]
        floats = x_in[3][...].reshape(512, 128).astype(F32)
        scale = floats[:, 0:1] + floats[:, 1:2] + floats[:, 2:3]
        arrived = x_in[j][...].reshape(512, width).astype(F32)
        arrived = (arrived * scale * fg[:, at : at + width]).astype(BF)
        g = dot(arrived, wg[at : at + width])
        u = dot(arrived, wu[at : at + width])
        if j == 0:
            acc_g[...] = g
            acc_u[...] = u
        elif j < count - 1:
            acc_g[...] += g
            acc_u[...] += u
        else:
            g = acc_g[...] + g
            act[...] = (g / (1.0 + jnp.exp(-g)) * (acc_u[...] + u)).astype(BF)

    def plane_out(j):
        for d in z_order:
            dz[j][d].wait_recv()
        y_out[j][...] = dot(turn, z_in[j][...]).astype(BF)
        for d in b_order:
            dy_[j][d].start()
        x_in[j][0, :16] = y_out[j][:16]

    def ring_out(j):
        for d in b_order:
            dy_[j][d].wait_recv()
        dx[j][0].start()
        dx[j][1].start()

    def ring_on(j):
        dx[j][0].wait_recv()
        dx[j][2].start()
        dx[j][1].wait_recv()
        dx[j][3].start()

    def ring_end(j):
        dx[j][2].wait_recv()
        dx[j][3].wait_recv()

    plane_out(0)
    plane_out(1)
    ring_out(0)
    plane_out(2)
    ring_out(1)
    ring_on(0)
    plane_out(3)
    ring_out(2)
    plane_out(4)
    ring_on(1)
    ring_out(3)
    ring_out(4)
    ring_on(2)
    ring_on(3)
    for load in loads[8:10]:
        load.wait()
    for j in range(4):
        ring_end(j)
    expert_in(0)
    ring_on(4)
    expert_in(1)
    expert_in(2)
    ring_end(4)
    expert_in(4)

    count = len(BACK)
    rx = [None] * count
    ry = [[None] * 8 for _ in range(count)]
    rz = [[None] * 8 for _ in range(count)]
    for j in range(count):
        rx[j] = (
            send(p_out[j].at[2, pl.ds(0, 64)], p_half[j].at[0], rxs.at[j, 0], rxr.at[j, 0], z, y, c, up),
            send(p_out[j].at[2, pl.ds(64, 64)], p_half[j].at[1], rxs.at[j, 1], rxr.at[j, 1], z, y, c, down),
            send(p_out[j].at[3], p_in[j].at[0], rxs.at[j, 2], rxr.at[j, 2], z, y, c, up),
            send(p_out[j].at[1], p_in[j].at[1], rxs.at[j, 3], rxr.at[j, 3], z, y, c, down),
        )
        for d in range(1, 8):
            py, pc = blocks[d]
            ry[j][d] = send(
                r_sum[j].at[b16(d)], ry_in[j].at[b16(d)], rys.at[j, d], ryr.at[j, d],
                z, yp(-py), (c + pc) % 2, x,
            )
            rz[j][d] = send(
                rz_out[j].at[b16(d)], rz_in[j].at[b16(d)], rzs.at[j, d], rzr.at[j, d],
                zp(-d), y, c, x,
            )
        all_sends += list(rx[j]) + ry[j][1:] + rz[j][1:]

    loads[10].wait()
    for t in range(count + 6):
        if t < count:
            at, width = BACK[t]
            part = dot(act[...], wd[:, at : at + width]).astype(BF)
            p_out[t][...] = part.reshape(4, 128, width)
            rx[t][0].start()
            rx[t][1].start()
        if 3 <= t <= count + 2:
            j = t - 3
            rx[j][2].wait_recv()
            rx[j][3].wait_recv()
            total = p_out[j][0].astype(F32) + p_in[j][0].astype(F32) + p_in[j][1].astype(F32)
            r_sum[j][...] = total.astype(BF)
            for d in b_order:
                ry[j][d].start()
            ry_in[j][:16] = r_sum[j][:16]
        if 4 <= t <= count + 3:
            j = t - 4
            for d in b_order:
                ry[j][d].wait_recv()
            rz_out[j][...] = dot(turn, ry_in[j][...]).astype(BF)
            for d in z_order:
                rz[j][d].start()
            rz_in[j][:16] = rz_out[j][:16]
        if 1 <= t <= count:
            j = t - 1
            rx[j][0].wait_recv()
            p_out[j][3, :64] = both(p_out[j][3, :64], p_half[j][0])
            rx[j][2].start()
            rx[j][1].wait_recv()
            p_out[j][1, 64:] = both(p_out[j][1, 64:], p_half[j][1])
            rx[j][3].start()
        if t >= 6:
            j = t - 6
            at, width = BACK[j]
            cols = slice(at, at + width)
            for d in z_order:
                rz[j][d].wait_recv()
            back = rz_in[j][...]
            mixed = col_w[0] * dot(picks[0], back) + col_w[1] * dot(picks[1], back)
            out_ref[:, cols] = (res[:, cols].astype(F32) + mixed).astype(BF)

    for s in all_sends:
        s.wait_send()


def body(
    query_a, query_b, latent, rope_key, latent_gain, key_a_weight, value_a_weight, key_b_weight,
    value_b_weight, out_a_weight, out_b_weight, residual, ffn_gain, routes, route_weight,
    expert_gate, expert_up, expert_down,
):
    hbm = pl.BlockSpec(memory_space=pltpu.HBM)
    dma = pltpu.SemaphoreType.DMA
    vm = pltpu.VMEM
    ta, tb = angle_tables()

    def pieces(columns, *rows):
        return [vm((*rows, width), BF) for _, width in columns]

    return pl.pallas_call(
        layer_kernel,
        out_shape=jax.ShapeDtypeStruct(residual.shape, BF),
        in_specs=[hbm] * 20,
        out_specs=pl.BlockSpec(memory_space=pltpu.VMEM),
        scratch_shapes=[
            vm((128, 384), BF), vm((128, 512), BF), vm((32, 512), BF), vm((32, 64), BF),
            vm((1, 512), F32), vm((32, 2048), BF), vm((1, 2048), F32),
            vm((2, 32), jnp.int32), vm((2, 32), F32), vm((64, 256), F32), vm((128, 256), F32),
            vm((32, 640), BF), vm((2, 128, 512), BF), vm((8, 256, 640), BF), vm((4, 256, 512), BF),
            vm((512, 512), BF), vm((2, 256, 2048), BF),
            vm((1024, 256), BF), vm((1024, 128), BF), vm((1024, 128), BF), vm((1024, 256), BF),
            vm((4, 256, 256), BF), vm((8, 128, 256), BF), vm((2, 8, 512), F32), vm((8, 8, 128), F32),
            vm((2, 3, 512, 128), F32), vm((2, 3, 512, 128), F32), vm((2, 3, 512, 128), F32),
            vm((4, 128, 512), BF), vm((4, 4, 32, 512), BF),
            vm((2048, 768), BF), vm((2048, 768), BF), vm((768, 2048), BF),
            pieces(OUT, 128), pieces(OUT, 128), pieces(OUT, 128), pieces(OUT, 4, 128),
            vm((512, 768), F32), vm((512, 768), F32), vm((512, 768), BF),
            pieces(BACK, 4, 128), pieces(BACK, 2, 64), pieces(BACK, 2, 128), pieces(BACK, 128),
            pieces(BACK, 128), pieces(BACK, 128), pieces(BACK, 128),
            dma((11,)), dma((11,)),
            dma((8,)), dma((8,)), dma((8, 4)), dma((8, 4)), dma((8,)), dma((8,)),
            dma((2, 5)), dma((2, 5)), dma((8,)), dma((8,)), dma((8,)), dma((8,)),
            dma((4, 4)), dma((4, 4)),
            dma((5, 8)), dma((5, 8)), dma((5, 8)), dma((5, 8)), dma((5, 4)), dma((5, 4)),
            dma((5, 4)), dma((5, 4)), dma((5, 8)), dma((5, 8)), dma((5, 8)), dma((5, 8)),
        ],
        compiler_params=pltpu.CompilerParams(
            collective_id=0, has_side_effects=True, vmem_limit_bytes=67043328
        ),
        cost_estimate=pl.CostEstimate(
            flops=2 * 10**10, bytes_accessed=2 * 10**7, transcendentals=10**7
        ),
    )(
        query_a, query_b, latent, rope_key, latent_gain.reshape(1, -1), key_a_weight,
        value_a_weight, key_b_weight, value_b_weight, out_a_weight, out_b_weight, residual,
        ffn_gain.reshape(1, -1), routes.T, route_weight.T, expert_gate, expert_up, expert_down,
        jnp.asarray(ta), jnp.asarray(tb),
    )


def solution(mesh):
    placed = (
        P("sp", "tp"),
        P("sp", "tp"),
        P(("sp", "tp"), None),
        P(("sp", "tp"), None),
        P(),
        P(None, "tp"),
        P(None, "tp"),
        P(None, "tp"),
        P(None, "tp"),
        P("tp", None),
        P("tp", None),
        P(("sp", "tp"), None),
        P(),
        P(("sp", "tp"), None),
        P(("sp", "tp"), None),
        P("sp", None, "tp"),
        P("sp", None, "tp"),
        P("sp", "tp", None),
    )
    return jax.shard_map(
        body, mesh=mesh, in_specs=placed, out_specs=P(("sp", "tp"), None), check_vma=False
    )
```

time: 149 us -> 125 us (0.84)
  Pallas kernels: 147 us -> 124 us
    pallas_call x1, Pallas kernels: 147 us -> 124 us  [body(): pl.pallas_call(layer_kernel, out_shape=jax.ShapeDtypeStruct(residual.shap...]
where the time goes in v2:
time: 125 us
  Pallas kernels  124 us (99%)
  local copies, waits for them, and re-layouts  1.57 us (1%)
    pallas_call x1, Pallas kernels, body(): pl.pallas_call(layer_kernel, out_shape=jax.ShapeDtypeStruct(residual.shap...  124 us

profile of v2, /device:TPU:1, one launch (start us, length us, event | category | flops | bytes accessed | tf_op | source)
XLA Modules:
  0.0 125.1 jit_solution(12511352883906630951)
XLA Ops:
  0.0 123.5 %shard_map.190 = bf16[32,2048]{1,0:T(8,128)(2,1)} custom-call(bf16[128,384]{1,0:T(8,128)(2,1)} %qa_ref.1, bf16[128,512]{1,0:T(8,128)(2,1)} %qb_ref.1, bf16[32,512]{1,0:T(8,128)(2,1)} %lat_ref.1, bf16[32,64]{1,0:T(8,128)(2,1)} %rope_ref.1, f32[1,512]{1,0:T(1,128)} %bitcast.5, bf16[512,256]{1,0:T(8,128)(2,1)} %ka_ref.1, bf16[512,256]{1,0:T(8,128)(2,1)} %va_ref.1, ...), custom_call_target="tpu_custom_call" | custom-call | flops 20000000000 | bytes 20000000 | tf_op jit(solution)/shard_map/pallas_call | solution.py:731
  123.6 1.6 %copy.22 = bf16[32,2048]{1,0:T(8,128)(2,1)} copy(bf16[32,2048]{1,0:T(8,128)(2,1)} %shard_map.190) | data formatting | bytes 262144

commit v3 on v2

--- a/solution.py
+++ b/solution.py
@@ -11,8 +11,8 @@
 NZ, NY, NX = 8, 4, 4
 TOKENS_PER_SP = 128
 ROWS = 32
-OUT = ((0, 512), (512, 512), (1024, 512), (None, 128), (1536, 512))
-BACK = ((0, 512), (512, 512), (1024, 512), (1536, 256), (1792, 256))
+OUT = ((0, 256), (256, 512), (768, 512), (1280, 512), (None, 128), (1792, 256))
+BACK = ((0, 256), (256, 512), (768, 512), (1280, 512), (1792, 256))
 LOG2E = 1.4426950408889634
 EPSILON = 1e-06
 BASE_THETA = 500000.0
@@ -376,52 +376,62 @@
     arrived_z(1)
     arrived_z(7)
     forward(0)
+    forward_q(0)
+    forward_q(1)
     arrived_z(2)
     forward(1)
-    to_mate(0)
-    forward_q(0)
     arrived_z(6)
     forward(7)
-    to_mate(1)
-    forward_q(1)
     arrived_z(3)
     forward(2)
-    to_mate(7)
     arrived_z(5)
     forward(6)
-    to_mate(2)
     arrived_z(4)
     forward(3)
-    to_mate(6)
+    to_mate(0)
+    to_mate(1)
     forward(5)
-    forward(4)
     for load in loads[:4]:
         load.wait()
     q_mate.wait_recv()
     for dc in range(2):
         q_sends[dc][2].wait_recv()
         q_sends[dc][3].wait_recv()
-    for i, d in enumerate((0, 1, 2, 7)):
+    for i, d in enumerate((0, 1)):
         m_sends[d].wait_recv()
-        if d < 2:
-            expand(i, d)
-        else:
-            pl.when(z >= d)(functools.partial(expand, i, d))
+        expand(i, d)
 
     def near(i, carried):
-        pl.when(z < 2)(functools.partial(attend, i, (0, 1)))
-        pl.when((z >= 2) & (z < 7))(functools.partial(attend, i, (0, 1, 2)))
-        pl.when(z == 7)(functools.partial(attend, i, (0, 1, 2, 7)))
+        attend(i, (0, 1))
 
         @pl.when(i == 0)
         def _():
+            to_mate(7)
+            to_mate(2)
+            forward(4)
+            to_mate(6)
+
+        return carried
+
+    lax.fori_loop(0, 2, near, 0)
+    for i, d in enumerate((2, 6, 7)):
+        m_sends[d].wait_recv()
+        pl.when(z >= d)(functools.partial(expand, i, d))
+
+    def middle(i, carried):
+        pl.when((z >= 2) & (z < 6))(functools.partial(attend, i, (2,)))
+        pl.when(z == 6)(functools.partial(attend, i, (2, 6)))
+        pl.when(z == 7)(functools.partial(attend, i, (2, 6, 7)))
+
+        @pl.when(i == 0)
+        def _():
+            to_mate(5)
             to_mate(3)
-            to_mate(5)
             to_mate(4)
 
         return carried
 
-    lax.fori_loop(0, 2, near, 0)
+    lax.fori_loop(0, 2, middle, 0)
 
     places = [(dy, dc) for dy in range(NY) for dc in range(2)]
     o_sends = [None] * 8
@@ -439,15 +449,14 @@
         )
     all_sends += o_sends[1:] + st_sends[1:]
 
-    for i, d in enumerate((3, 4, 5, 6)):
+    for i, d in enumerate((3, 4, 5)):
         m_sends[d].wait_recv()
         pl.when(z >= (3 if d == 4 else d))(functools.partial(expand, i, d))
 
     def far(t, carried):
         i = 1 - t
         pl.when((z == 3) | (z == 4))(functools.partial(attend, i, (3, 4)))
-        pl.when(z == 5)(functools.partial(attend, i, (3, 4, 5)))
-        pl.when(z >= 6)(functools.partial(attend, i, (3, 4, 5, 6)))
+        pl.when(z >= 5)(functools.partial(attend, i, (3, 4, 5)))
         finish(i)
 
         @pl.when(t == 0)
@@ -495,16 +504,16 @@
     def both(a, b):
         return (a.astype(F32) + b.astype(F32)).astype(BF)
 
-    p_sends = []
-    for j in range(4):
-        cols = slice(j * 512, j * 512 + 512)
-        pj[j] = (dot(made[0], wo[0, :, cols]) + dot(made[1], wo[1, :, cols])).astype(BF)
-        p_sends.append(
-            [
-                send(pj.at[j, rows_to(d)], pj_in.at[j, d], ps.at[j, d], pr.at[j, d], z, y, c, xp(d))
-                for d in (2, 1, 3)
-            ]
-        )
+    data = [j for j, (at, _) in enumerate(OUT) if at is not None]
+    scaled = len(OUT) - 2
+    p_sends = {}
+    for j in data:
+        cols = slice(OUT[j][0], sum(OUT[j]))
+        pj[j][...] = (dot(made[0], wo[0, :, cols]) + dot(made[1], wo[1, :, cols])).astype(BF)
+        p_sends[j] = [
+            send(pj[j].at[rows_to(d)], pj_in[j].at[d], ps.at[j, d], pr.at[j, d], z, y, c, xp(d))
+            for d in (2, 1, 3)
+        ]
         for s in p_sends[j]:
             s.start()
         all_sends += p_sends[j]
@@ -531,18 +540,25 @@
                 z, yp(py), (c + pc) % 2, x,
             )
         top_half, low_half = pl.ds(0, 64), pl.ds(64, 64)
-        dx[j] = (
+        dx[j] = [
             send(x_in[j].at[0], x_in[j].at[1], dxs.at[j, 0], dxr.at[j, 0], z, y, c, up),
             send(x_in[j].at[0], x_in[j].at[3], dxs.at[j, 1], dxr.at[j, 1], z, y, c, down),
-            send(
-                x_in[j].at[1, top_half], x_in[j].at[2, top_half],
-                dxs.at[j, 2], dxr.at[j, 2], z, y, c, up,
-            ),
-            send(
-                x_in[j].at[3, low_half], x_in[j].at[2, low_half],
-                dxs.at[j, 3], dxr.at[j, 3], z, y, c, down,
-            ),
-        )
+        ]
+        if j == scaled:
+            dx[j].append(
+                send(x_in[j].at[0], x_in[j].at[2], dxs.at[j, 2], dxr.at[j, 2], z, y, c, xp(2))
+            )
+        else:
+            dx[j] += [
+                send(
+                    x_in[j].at[1, top_half], x_in[j].at[2, top_half],
+                    dxs.at[j, 2], dxr.at[j, 2], z, y, c, up,
+                ),
+                send(
+                    x_in[j].at[3, low_half], x_in[j].at[2, low_half],
+                    dxs.at[j, 3], dxr.at[j, 3], z, y, c, down,
+                ),
+            ]
         all_sends += dz[j][1:] + dy_[j][1:] + list(dx[j])
 
     def dispatch(j, rows):
@@ -552,20 +568,18 @@
         z_in[j][:16] = disp[j][:16]
 
     squares = jnp.zeros((ROWS, 1), F32)
-    for j in range(4):
-        cols = slice(j * 512, j * 512 + 512)
-        total = res[:, cols].astype(F32) + pj[j, rows_to(0)].astype(F32)
+    for j in data:
+        cols = slice(OUT[j][0], sum(OUT[j]))
+        total = res[:, cols].astype(F32) + pj[j][rows_to(0)].astype(F32)
         for s in p_sends[j]:
             s.wait_recv()
         for d in range(1, NX):
-            total = total + pj_in[j, d].astype(F32)
+            total = total + pj_in[j][d].astype(F32)
         hidden = total.astype(BF)
         res[:, cols] = hidden
         total = hidden.astype(F32)
         squares = squares + jnp.sum(total * total, axis=1, keepdims=True)
-        if j < 3:
-            dispatch(j, hidden)
-        else:
+        if j > scaled:
             exact = lax.rsqrt(squares * (1.0 / 2048) + EPSILON)
             terms = []
             for _ in range(3):
@@ -575,12 +589,12 @@
             scales = jnp.zeros((ROWS, 128), F32)
             for k in range(3):
                 scales = jnp.where(lane == k, terms[k].astype(F32), scales)
-            dispatch(3, scales.astype(BF))
-            dispatch(4, hidden)
+            dispatch(scaled, scales.astype(BF))
+        dispatch(j, hidden)
 
     def expert_in(j):
         at, width = OUT[j]
-        floats = x_in[3][...].reshape(512, 128).astype(F32)
+        floats = x_in[scaled][...].reshape(512, 128).astype(F32)
         scale = floats[:, 0:1] + floats[:, 1:2] + floats[:, 2:3]
         arrived = x_in[j][...].reshape(512, width).astype(F32)
         arrived = (arrived * scale * fg[:, at : at + width]).astype(BF)
@@ -607,8 +621,8 @@
     def ring_out(j):
         for d in b_order:
             dy_[j][d].wait_recv()
-        dx[j][0].start()
-        dx[j][1].start()
+        for s in dx[j] if j == scaled else dx[j][:2]:
+            s.start()
 
     def ring_on(j):
         dx[j][0].wait_recv()
@@ -616,34 +630,24 @@
         dx[j][1].wait_recv()
         dx[j][3].start()
 
-    def ring_end(j):
+    def scale_in(j):
+        for s in dx[j]:
+            s.wait_recv()
+        for load in loads[8:10]:
+            load.wait()
+
+    def expert(j):
         dx[j][2].wait_recv()
         dx[j][3].wait_recv()
-
-    plane_out(0)
-    plane_out(1)
-    ring_out(0)
-    plane_out(2)
-    ring_out(1)
-    ring_on(0)
-    plane_out(3)
-    ring_out(2)
-    plane_out(4)
-    ring_on(1)
-    ring_out(3)
-    ring_out(4)
-    ring_on(2)
-    ring_on(3)
-    for load in loads[8:10]:
-        load.wait()
-    for j in range(4):
-        ring_end(j)
-    expert_in(0)
-    ring_on(4)
-    expert_in(1)
-    expert_in(2)
-    ring_end(4)
-    expert_in(4)
+        expert_in(j)
+
+    for step, j in (
+        (plane_out, 0), (plane_out, 1), (ring_out, 0), (plane_out, 2), (ring_out, 1), (ring_on, 0),
+        (plane_out, 3), (ring_out, 2), (plane_out, 4), (plane_out, 5), (ring_on, 1), (ring_out, 4),
+        (ring_out, 3), (ring_out, 5), (ring_on, 2), (scale_in, 4), (expert, 0), (expert, 1),
+        (ring_on, 3), (ring_on, 5), (expert, 2), (expert, 3), (expert, 5),
+    ):
+        step(j)
 
     count = len(BACK)
     rx = [None] * count
@@ -739,10 +743,10 @@
             vm((2, 32), jnp.int32), vm((2, 32), F32), vm((64, 256), F32), vm((128, 256), F32),
             vm((32, 640), BF), vm((2, 128, 512), BF), vm((8, 256, 640), BF), vm((4, 256, 512), BF),
             vm((512, 512), BF), vm((2, 256, 2048), BF),
-            vm((1024, 256), BF), vm((1024, 128), BF), vm((1024, 128), BF), vm((1024, 256), BF),
+            vm((768, 256), BF), vm((768, 128), BF), vm((768, 128), BF), vm((768, 256), BF),
             vm((4, 256, 256), BF), vm((8, 128, 256), BF), vm((2, 8, 512), F32), vm((8, 8, 128), F32),
             vm((2, 3, 512, 128), F32), vm((2, 3, 512, 128), F32), vm((2, 3, 512, 128), F32),
-            vm((4, 128, 512), BF), vm((4, 4, 32, 512), BF),
+            pieces(OUT, 128), pieces(OUT, 4, 32),
             vm((2048, 768), BF), vm((2048, 768), BF), vm((768, 2048), BF),
             pieces(OUT, 128), pieces(OUT, 128), pieces(OUT, 128), pieces(OUT, 4, 128),
             vm((512, 768), F32), vm((512, 768), F32), vm((512, 768), BF),
@@ -751,9 +755,9 @@
             dma((11,)), dma((11,)),
             dma((8,)), dma((8,)), dma((8, 4)), dma((8, 4)), dma((8,)), dma((8,)),
             dma((2, 5)), dma((2, 5)), dma((8,)), dma((8,)), dma((8,)), dma((8,)),
-            dma((4, 4)), dma((4, 4)),
-            dma((5, 8)), dma((5, 8)), dma((5, 8)), dma((5, 8)), dma((5, 4)), dma((5, 4)),
-            dma((5, 4)), dma((5, 4)), dma((5, 8)), dma((5, 8)), dma((5, 8)), dma((5, 8)),
+            dma((6, 4)), dma((6, 4)),
+            dma((6, 8)), dma((6, 8)), dma((6, 8)), dma((6, 8)), dma((6, 4)), dma((6, 4)),
+            dma((6, 4)), dma((6, 4)), dma((6, 8)), dma((6, 8)), dma((6, 8)), dma((6, 8)),
         ],
         compiler_params=pltpu.CompilerParams(
             collective_id=0, has_side_effects=True, vmem_limit_bytes=67043328

time: 125 us -> 122 us (0.976)
  Pallas kernels: 124 us -> 120 us
    pallas_call x1, Pallas kernels: 124 us -> 120 us  [body(): pl.pallas_call(layer_kernel, out_shape=jax.ShapeDtypeStruct(residual.shap...]
where the time goes in v3:
time: 122 us
  Pallas kernels  120 us (98%)
  local copies, waits for them, and re-layouts  1.57 us (1%)
    pallas_call x1, Pallas kernels, body(): pl.pallas_call(layer_kernel, out_shape=jax.ShapeDtypeStruct(residual.shap...  120 us

profile of v3, /device:TPU:1, one launch (start us, length us, event | category | flops | bytes accessed | tf_op | source)
XLA Modules:
  0.0 121.6 jit_solution(3114608616243816930)
XLA Ops:
  0.0 120.1 %shard_map.190 = bf16[32,2048]{1,0:T(8,128)(2,1)} custom-call(bf16[128,384]{1,0:T(8,128)(2,1)} %qa_ref.1, bf16[128,512]{1,0:T(8,128)(2,1)} %qb_ref.1, bf16[32,512]{1,0:T(8,128)(2,1)} %lat_ref.1, bf16[32,64]{1,0:T(8,128)(2,1)} %rope_ref.1, f32[1,512]{1,0:T(1,128)} %bitcast.5, bf16[512,256]{1,0:T(8,128)(2,1)} %ka_ref.1, bf16[512,256]{1,0:T(8,128)(2,1)} %va_ref.1, ...), custom_call_target="tpu_custom_call" | custom-call | flops 20000000000 | bytes 20000000 | tf_op jit(solution)/shard_map/pallas_call | solution.py:735
  120.1 1.6 %copy.22 = bf16[32,2048]{1,0:T(8,128)(2,1)} copy(bf16[32,2048]{1,0:T(8,128)(2,1)} %shard_map.190) | data formatting | bytes 262144

commit v4 on v3

--- a/solution.py
+++ b/solution.py
@@ -109,7 +109,7 @@
             )
     for i, (src, dst) in enumerate(((eg_ref, wg), (eu_ref, wu), (ed_ref, wd))):
         loads.append(pltpu.make_async_copy(src.at[0], dst, w_sem.at[8 + i]))
-    for load in loads:
+    for load in loads[:4]:
         load.start()
 
     barrier = pltpu.get_barrier_semaphore()
@@ -230,6 +230,8 @@
         q_sends[dc][0].start()
         q_sends[dc][1].start()
     q_mate.start()
+    for load in loads[4:]:
+        load.start()
     qg[0, core_rows] = q_own[c]
 
     m_sends = [
@@ -248,46 +250,6 @@
         x_sends[d][2].wait_recv()
         x_sends[d][3].wait_recv()
         m_sends[d].start()
-
-    for load in small[7:]:
-        load.wait()
-    eye = iota((32, 32), 0) == iota((32, 32), 1)
-    before = iota((32, 32), 1) < iota((32, 32), 0)
-    after = iota((32, 32), 0) < iota((32, 32), 1)
-    chosen = rt[...]
-    row_e = [chosen[k : k + 1].astype(F32) for k in range(2)]
-    col_e = [jnp.sum(jnp.where(eye, e, 0.0), axis=1, keepdims=True) for e in row_e]
-    share = wt[...]
-    col_w = [
-        jnp.sum(jnp.where(eye, share[k : k + 1], 0.0), axis=1, keepdims=True) for k in range(2)
-    ]
-
-    def slot(e, rank):
-        e = e.astype(jnp.int32)
-        dz = (e // 8 - z + NZ) % NZ
-        dy = ((e // 2) % 4 - y + NY) % NY
-        dc = (e % 2 - c + 2) % 2
-        return dz * 16 + dy * 4 + dc * 2 + rank.astype(jnp.int32)
-
-    row_slot, col_slot = [], []
-    for k in range(2):
-        rank_row = jnp.zeros((1, 32), F32)
-        rank_col = jnp.zeros((32, 1), F32)
-        for o in range(2):
-            same = (col_e[o] == row_e[k]) & after
-            rank_row = rank_row + jnp.sum(jnp.where(same, 1.0, 0.0), axis=0, keepdims=True)
-            same = (row_e[o] == col_e[k]) & before
-            rank_col = rank_col + jnp.sum(jnp.where(same, 1.0, 0.0), axis=1, keepdims=True)
-        row_slot.append(slot(row_e[k], rank_row))
-        col_slot.append(slot(col_e[k], rank_col))
-    s_row = iota((128, 32), 0)
-    chosen_rows = ((s_row == row_slot[0]) | (s_row == row_slot[1])).astype(BF)
-    s_lane = iota((32, 128), 1)
-    picks = [(s_lane == col_slot[k]).astype(BF) for k in range(2)]
-    out_at, in_at = iota((128, 128), 0), iota((128, 128), 1)
-    turn = (
-        in_at == ((out_at // 2) % 8) * 16 + (out_at // 16) * 2 + out_at % 2
-    ).astype(BF)
 
     lane = iota((256, 128), 1)
     lane_512 = iota((512, 128), 1)
@@ -471,6 +433,46 @@
     for k in (2, 3, 1):
         o_sends[k].start()
         st_sends[k].start()
+    for load in small[7:]:
+        load.wait()
+    eye = iota((32, 32), 0) == iota((32, 32), 1)
+    before = iota((32, 32), 1) < iota((32, 32), 0)
+    after = iota((32, 32), 0) < iota((32, 32), 1)
+    chosen = rt[...]
+    row_e = [chosen[k : k + 1].astype(F32) for k in range(2)]
+    col_e = [jnp.sum(jnp.where(eye, e, 0.0), axis=1, keepdims=True) for e in row_e]
+    share = wt[...]
+    col_w = [
+        jnp.sum(jnp.where(eye, share[k : k + 1], 0.0), axis=1, keepdims=True) for k in range(2)
+    ]
+
+    def slot(e, rank):
+        e = e.astype(jnp.int32)
+        dz = (e // 8 - z + NZ) % NZ
+        dy = ((e // 2) % 4 - y + NY) % NY
+        dc = (e % 2 - c + 2) % 2
+        return dz * 16 + dy * 4 + dc * 2 + rank.astype(jnp.int32)
+
+    row_slot, col_slot = [], []
+    for k in range(2):
+        rank_row = jnp.zeros((1, 32), F32)
+        rank_col = jnp.zeros((32, 1), F32)
+        for o in range(2):
+            same = (col_e[o] == row_e[k]) & after
+            rank_row = rank_row + jnp.sum(jnp.where(same, 1.0, 0.0), axis=0, keepdims=True)
+            same = (row_e[o] == col_e[k]) & before
+            rank_col = rank_col + jnp.sum(jnp.where(same, 1.0, 0.0), axis=1, keepdims=True)
+        row_slot.append(slot(row_e[k], rank_row))
+        col_slot.append(slot(col_e[k], rank_col))
+    s_row = iota((128, 32), 0)
+    chosen_rows = ((s_row == row_slot[0]) | (s_row == row_slot[1])).astype(BF)
+    s_lane = iota((32, 128), 1)
+    picks = [(s_lane == col_slot[k]).astype(BF) for k in range(2)]
+    out_at, in_at = iota((128, 128), 0), iota((128, 128), 1)
+    turn = (
+        in_at == ((out_at // 2) % 8) * 16 + (out_at // 16) * 2 + out_at % 2
+    ).astype(BF)
+
     for load in loads[4:8]:
         load.wait()
     for k in range(1, 8):

time: 122 us -> 122 us (level)
  no operation moved by 1% of the time
where the time goes in v4:
time: 122 us
  Pallas kernels  120 us (98%)
  local copies, waits for them, and re-layouts  1.57 us (1%)
    pallas_call x1, Pallas kernels, body(): pl.pallas_call(layer_kernel, out_shape=jax.ShapeDtypeStruct(residual.shap...  120 us

profile of v4, /device:TPU:1, one launch (start us, length us, event | category | flops | bytes accessed | tf_op | source)
XLA Modules:
  0.0 121.5 jit_solution(2493480066179636021)
XLA Ops:
  0.0 120.0 %shard_map.190 = bf16[32,2048]{1,0:T(8,128)(2,1)} custom-call(bf16[128,384]{1,0:T(8,128)(2,1)} %qa_ref.1, bf16[128,512]{1,0:T(8,128)(2,1)} %qb_ref.1, bf16[32,512]{1,0:T(8,128)(2,1)} %lat_ref.1, bf16[32,64]{1,0:T(8,128)(2,1)} %rope_ref.1, f32[1,512]{1,0:T(1,128)} %bitcast.5, bf16[512,256]{1,0:T(8,128)(2,1)} %ka_ref.1, bf16[512,256]{1,0:T(8,128)(2,1)} %va_ref.1, ...), custom_call_target="tpu_custom_call" | custom-call | flops 20000000000 | bytes 20000000 | tf_op jit(solution)/shard_map/pallas_call | solution.py:737
  120.0 1.6 %copy.22 = bf16[32,2048]{1,0:T(8,128)(2,1)} copy(bf16[32,2048]{1,0:T(8,128)(2,1)} %shard_map.190) | data formatting | bytes 262144
